TPU v7x, 512 devices: a whole 4x8x8 slice. The times are simulated.
512 devices in a mesh: sp: 64 (over z, y), tp: 8 (over x, core).
Axes of the slice: x: 4, y: 8, z: 8, core: 2. Of those that a mesh axis runs over, the one named last changes fastest.
Arguments:
- tokens: bfloat16 [8192, 2048], P('sp', 'tp'), may hold values from -6 to 6
- pre_gain: float32 [2048], replicated, may hold values from 0.1 to 1.9
- w_query_stick: bfloat16 [2048, 1024], P(None, 'tp'), may hold values from -0.125 to 0.125
- w_key_stick: bfloat16 [2048, 1024], P(None, 'tp'), may hold values from -0.125 to 0.125
- w_value_stick: bfloat16 [2048, 1024], P(None, 'tp'), may hold values from -2 to 2, as said below
- w_query_window: bfloat16 [2048, 1024], P(None, 'tp'), may hold values from -20 to 20, as said below
- w_key_window: bfloat16 [2048, 512], P(None, 'tp'), may hold values from -1 to 1, as said below
- w_value_window: bfloat16 [2048, 512], P(None, 'tp'), may hold values from -2 to 2, as said below
- stick_bias: float32 [16], P('tp'), may hold values from -14 to -3
- sinks: float32 [16], P('tp'), may hold values from 2 to 6
- stick_gain: float32 [1024], P('tp'), may hold values from 0.1 to 1.9
- window_gain: float32 [1024], P('tp'), may hold values from 0.1 to 1.9
- w_out_stick: bfloat16 [1024, 2048], P('tp'), may hold values from -0.125 to 0.125
- w_out_window: bfloat16 [1024, 2048], P('tp'), may hold values from -0.125 to 0.125
- post_gain: float32 [2048], replicated, may hold values from 0.1 to 1.9
Outputs:
- layer_out: bfloat16 [8192, 2048], P(('sp', 'tp'))
Inputs may be any that keep to these rules, and one draw needn't show every extreme that they name: `w_key_window`: key weights of the windowed heads. `w_query_window`: query weights of the windowed heads. `w_value_stick`: value weights of the stick-breaking heads. `w_value_window`: value weights of the windowed heads.
All inputs are finite; a program needn't handle non-finite values.
Results may differ from a plain program's by a relative error of at most 0.018.
Values may be sent and summed in bfloat16 or wider, within the bound.
A program may use at most 64 MiB of HBM per device.

v0:
```python
import jax
import jax.numpy as jnp
from jax import lax
from jax.sharding import PartitionSpec as P

HEAD_DIM = 64
GROUP = 2
WINDOW = 128
SB_WIDTH = 1024
SW_WIDTH = 1024


epsilon = 1e-06


def laid_out(tiles, dim):
    tiles = jnp.moveaxis(tiles, 0, dim)
    shape = tiles.shape
    return tiles.reshape(*shape[:dim], shape[dim] * shape[dim + 1], *shape[dim + 2 :])


def from_everyone(array, axis):
    size = lax.axis_size(axis)
    return lax.all_to_all(
        jnp.broadcast_to(array[None], (size, *array.shape)), axis, 0, 0, tiled=True
    )


def gathered_copies(array, axis, dim):
    return laid_out(from_everyone(array, axis), dim)


def passed_along(value, axis, steps):
    count = lax.axis_size(axis)
    initial, last = (max(0, -steps), min(count, count - steps))
    return lax.ppermute(value, axis, [(source, source + steps) for source in range(initial, last)])


def over_copies(array, axis):
    return from_everyone(array, axis).sum(axis=0)


def packed_total(arrays, axis):
    flat, at, outs = (jnp.concatenate([a.reshape(-1) for a in arrays]), 0, [])
    subtotal = over_copies(flat, axis)
    for a in arrays:
        outs.append(subtotal[at : at + a.size].reshape(a.shape))
        at += a.size
    return tuple(outs)


def rounded(values):
    return lax.optimization_barrier(values.astype(jnp.bfloat16)).astype(jnp.float32)


def norm_rows(values, gain):
    stats = jnp.mean(values * values, axis=-1, keepdims=True)
    return values * lax.rsqrt(stats + epsilon) * gain


def stick_block(queries, key_pair, head_bias, key_mask, carried):
    result, logsum = carried
    head_count = queries.shape[1]
    key_rows = key_pair[0].reshape(key_pair.shape[1], head_count, HEAD_DIM)
    values = key_pair[1].reshape(key_pair.shape[1], head_count, HEAD_DIM)
    scores = jnp.einsum(
        "thd,shd->hts", queries, key_rows, preferred_element_type=jnp.float32
    ) * HEAD_DIM ** (-0.5)
    scores = scores + head_bias[:, None, None]
    usable = key_mask[None]
    log_keep = jnp.where(usable, jax.nn.log_sigmoid(-scores), 0.0)
    suffix = lax.cumsum(log_keep, axis=2, reverse=True) - log_keep
    stick_weights = jnp.where(
        usable, jnp.exp(jax.nn.log_sigmoid(scores) + suffix + logsum[:, :, None]), 0.0
    )
    stick_weights = stick_weights.astype(jnp.bfloat16)
    result = result + jnp.einsum(
        "hts,shd->htd", stick_weights, values, preferred_element_type=jnp.float32
    )
    logsum = logsum + jnp.sum(log_keep, axis=2)
    return (result, logsum)


def shards(
    tokens,
    pre_gain,
    w_query_stick,
    w_key_stick,
    w_value_stick,
    w_query_window,
    w_key_window,
    w_value_window,
    stick_bias,
    sinks,
    stick_gain,
    window_gain,
    w_out_stick,
    w_out_window,
    post_gain,
):
    gathered = gathered_copies(tokens, "tp", 1)
    normed = norm_rows(gathered.astype(jnp.float32), pre_gain).astype(jnp.bfloat16)

    def project(weight):
        return jnp.dot(normed, weight, preferred_element_type=jnp.float32).astype(jnp.bfloat16)

    tok_rows = normed.shape[0]
    dev_index = lax.axis_index("sp")
    dev_count = lax.axis_size("sp")
    query_stick = project(w_query_stick)
    stick_heads = query_stick.shape[1] // HEAD_DIM
    queries = query_stick.reshape(tok_rows, stick_heads, HEAD_DIM)
    own_pair = jnp.stack([project(w_key_stick), project(w_value_stick)])
    pair_width = own_pair.shape[2]
    positions = jnp.arange(tok_rows, dtype=jnp.int32)
    initial = (
        jnp.zeros((stick_heads, tok_rows, HEAD_DIM), jnp.float32),
        jnp.zeros((stick_heads, tok_rows), jnp.float32),
    )
    collected = own_pair[None]
    for section_index in range(dev_count.bit_length() - 1):
        arrived = passed_along(collected, "sp", 2**section_index)
        collected = jnp.concatenate([arrived, collected], axis=0)
    per_group = min(dev_count, 8)
    group_count = dev_count // per_group
    grouped = collected.reshape(group_count, per_group, 2, tok_rows, pair_width)
    grouped = grouped.transpose(0, 2, 1, 3, 4).reshape(
        group_count, 2, per_group * tok_rows, pair_width
    )
    first_source = dev_index - (dev_count - 1)
    group_starts = (first_source + jnp.arange(group_count, dtype=jnp.int32) * per_group) * tok_rows
    query_pos = dev_index * tok_rows + positions
    span_offs = jnp.arange(per_group * tok_rows, dtype=jnp.int32)

    def visit_group(carried, inputs):
        key_pair, start_pos = inputs
        key_pos = start_pos + span_offs
        key_mask = (key_pos[None, :] >= 0) & (key_pos[None, :] < query_pos[:, None])
        return (stick_block(queries, key_pair, stick_bias, key_mask, carried), None)

    (stick_sum, _), _ = lax.scan(visit_group, initial, (grouped, group_starts), reverse=True)
    stick_out = (
        stick_sum.transpose(1, 0, 2).reshape(tok_rows, stick_heads * HEAD_DIM).astype(jnp.bfloat16)
    )
    query_window = project(w_query_window)
    window_pair = jnp.stack([project(w_key_window), project(w_value_window)])
    kv_heads = window_pair.shape[2] // HEAD_DIM
    previous = passed_along(window_pair, "sp", 1)
    extended = jnp.concatenate([previous, window_pair], axis=1)
    block_count = tok_rows // WINDOW
    extended = extended.reshape(2, block_count + 1, WINDOW, kv_heads, HEAD_DIM)
    banded = jnp.concatenate([extended[:, :-1], extended[:, 1:]], axis=2)
    q_blocks = query_window.reshape(block_count, WINDOW, kv_heads, GROUP, HEAD_DIM)
    logits = jnp.einsum(
        "nqhgd,nchd->nhgqc", q_blocks, banded[0], preferred_element_type=jnp.float32
    ) * HEAD_DIM ** (-0.5)
    query_offs = jnp.arange(WINDOW, dtype=jnp.int32)[:, None]
    key_offs = jnp.arange(2 * WINDOW, dtype=jnp.int32)[None, :]
    distance = query_offs + WINDOW - key_offs
    key_pos = (
        dev_index * tok_rows
        + jnp.arange(block_count, dtype=jnp.int32)[:, None] * WINDOW
        - WINDOW
        + key_offs
    )
    usable = ((distance >= 0) & (distance < WINDOW))[None] & (key_pos >= 0)[:, None, :]
    logits = jnp.where(usable[:, None, None], logits, -jnp.inf)
    sink_logit = sinks.reshape(kv_heads, GROUP)[None, :, :, None, None]
    row_top = jnp.maximum(jnp.max(logits, axis=-1, keepdims=True), sink_logit)
    weights_exp = jnp.exp(logits - row_top)
    normalizer = jnp.sum(weights_exp, axis=-1, keepdims=True) + jnp.exp(sink_logit - row_top)
    window_weights = (weights_exp / normalizer).astype(jnp.bfloat16)
    window_sum = jnp.einsum(
        "nhgqc,nchd->nqhgd", window_weights, banded[1], preferred_element_type=jnp.float32
    )
    window_out = window_sum.reshape(tok_rows, query_window.shape[1]).astype(jnp.bfloat16)
    stick_float = stick_out.astype(jnp.float32)
    window_float = window_out.astype(jnp.float32)
    squares = packed_total(
        (jnp.sum(stick_float * stick_float, axis=1), jnp.sum(window_float * window_float, axis=1)),
        "tp",
    )
    stick_normed = (
        stick_float * lax.rsqrt(squares[0][:, None] / SB_WIDTH + epsilon) * stick_gain
    ).astype(jnp.bfloat16)
    window_normed = (
        window_float * lax.rsqrt(squares[1][:, None] / SW_WIDTH + epsilon) * window_gain
    ).astype(jnp.bfloat16)
    total = jnp.dot(stick_normed, w_out_stick, preferred_element_type=jnp.float32)
    combined = lax.psum_scatter(
        (total + jnp.dot(window_normed, w_out_window, preferred_element_type=jnp.float32)).astype(
            jnp.bfloat16
        ),
        "tp",
        scatter_dimension=0,
        tiled=True,
    ).astype(jnp.float32)
    combined = rounded(combined)
    return norm_rows(combined, post_gain).astype(jnp.bfloat16)


def solution(mesh):
    in_specs = (
        P("sp", "tp"),
        P(),
        P(None, "tp"),
        P(None, "tp"),
        P(None, "tp"),
        P(None, "tp"),
        P(None, "tp"),
        P(None, "tp"),
        P("tp"),
        P("tp"),
        P("tp"),
        P("tp"),
        P("tp", None),
        P("tp", None),
        P(),
    )
    out_specs = P(("sp", "tp"), None)
    return jax.shard_map(shards, mesh=mesh, in_specs=in_specs, out_specs=out_specs, check_vma=False)
```

profile of v0, /device:TPU:8, one launch (start us, length us, event | category | flops | bytes accessed | tf_op | source)
XLA Modules:
  0.0 461.1 jit_solution(8751095200928946585)
XLA Ops:
  6.5 1.0 copy.42
  7.7 14.5 %all_to_all.11 = bf16[8,128,256]{1,2,0:T(8,128)(2,1)S(1)} all-to-all(bf16[8,128,256]{1,2,0:T(8,128)(2,1)S(1)} %broadcast_in_dim.51), channel_id=1, replica_groups=mesh['sp'=64,'tp'=8] {'tp'}, dimensions={0} | all-to-all | bytes 1048576 | tf_op jit(solution)/shard_map/all_to_all | solution.py:24
  22.4 1.0 fusion.26
  23.5 1.4 fusion.22
  25.2 3.5 collective-permute-start
  28.7 4.1 collective-permute-done
  32.9 3.5 collective-permute-start.1
  36.3 2.5 collective-permute-done.1
  38.9 10.8 %collective-permute-start.2 = (bf16[4,2,128,128]{3,2,1,0:T(8,128)(2,1)S(1)}, bf16[4,2,128,128]{3,2,1,0:T(8,128)(2,1)S(1)}, u32[]{:S(2)}, u32[]{:S(2)}) collective-permute-start(bf16[4,2,128,128]{3,2,1,0:T(8,128)(2,1)S(1)} %pad_maximum_fusion.1), channel_id=1, source_target_pairs={{0,32},{8,40},{16,48},{24,56},{32,64},{40,72},{48,80},{56,88},{64,... | collective-permute-start | bytes 786440 | tf_op jit(solution)/shard_map/ppermute | solution.py:36
  49.7 4.7 %collective-permute-done.2 = bf16[4,2,128,128]{3,2,1,0:T(8,128)(2,1)S(1)} collective-permute-done((bf16[4,2,128,128]{3,2,1,0:T(8,128)(2,1)S(1)}, bf16[4,2,128,128]{3,2,1,0:T(8,128)(2,1)S(1)}, u32[]{:S(2)}, u32[]{:S(2)}) %collective-permute-start.2) | collective-permute-done | bytes 262176 | tf_op jit(solution)/shard_map/ppermute | solution.py:36
  54.4 7.6 %collective-permute-start.3 = (bf16[8,2,128,128]{3,2,1,0:T(8,128)(2,1)S(1)}, bf16[8,2,128,128]{3,2,1,0:T(8,128)(2,1)S(1)}, u32[]{:S(2)}, u32[]{:S(2)}) collective-permute-start(bf16[8,2,128,128]{3,2,1,0:T(8,128)(2,1)S(1)} %pad_maximum_fusion), channel_id=1, source_target_pairs={{0,64},{8,72},{16,80},{24,88},{32,96},{40,104},{48,112},{56,120},{... | collective-permute-start | bytes 1572872 | tf_op jit(solution)/shard_map/ppermute | solution.py:36
  62.1 7.5 %collective-permute-done.3 = bf16[8,2,128,128]{3,2,1,0:T(8,128)(2,1)S(1)} collective-permute-done((bf16[8,2,128,128]{3,2,1,0:T(8,128)(2,1)S(1)}, bf16[8,2,128,128]{3,2,1,0:T(8,128)(2,1)S(1)}, u32[]{:S(2)}, u32[]{:S(2)}) %collective-permute-start.3) | collective-permute-done | bytes 524320 | tf_op jit(solution)/shard_map/ppermute | solution.py:36
  73.1 6.2 %collective-permute-start.4 = (bf16[16,2,128,128]{3,2,1,0:T(8,128)(2,1)}, bf16[16,2,128,128]{3,2,1,0:T(8,128)(2,1)S(1)}, u32[]{:S(2)}, u32[]{:S(2)}) collective-permute-start(bf16[16,2,128,128]{3,2,1,0:T(8,128)(2,1)} %constant_dynamic-update-slice_fusion), channel_id=1, source_target_pairs={{0,128},{8,136},{16,144},{24,152},{32,160},{40,168},{48,176},{56,1... | collective-permute-start | bytes 3145736 | tf_op jit(solution)/shard_map/ppermute | solution.py:36
  79.7 1.2 fusion.24
  80.9 1.4 convolution_convert_fusion.1
  82.3 15.2 %collective-permute-done.4 = bf16[16,2,128,128]{3,2,1,0:T(8,128)(2,1)S(1)} collective-permute-done((bf16[16,2,128,128]{3,2,1,0:T(8,128)(2,1)}, bf16[16,2,128,128]{3,2,1,0:T(8,128)(2,1)S(1)}, u32[]{:S(2)}, u32[]{:S(2)}) %collective-permute-start.4) | collective-permute-done | bytes 1048608 | tf_op jit(solution)/shard_map/ppermute | solution.py:36
  97.5 1.1 constant_dynamic-update-slice_fusion.10
  98.6 0.9 constant_dynamic-update-slice_fusion.9
  102.0 42.8 %collective-permute-start.5 = (bf16[32,2,128,128]{3,2,1,0:T(8,128)(2,1)}, bf16[32,2,128,128]{3,2,1,0:T(8,128)(2,1)}, u32[]{:S(2)}, u32[]{:S(2)}) collective-permute-start(bf16[32,2,128,128]{3,2,1,0:T(8,128)(2,1)} %constant_dynamic-update-slice_fusion.5), channel_id=1, source_target_pairs={{0,256},{8,264},{16,272},{24,280},{32,288},{40,296},{48,304},{56,3... | collective-permute-start | bytes 6291464 | tf_op jit(solution)/shard_map/ppermute | solution.py:36
  144.9 19.2 %collective-permute-start.6 = (bf16[2,128,64]{1,2,0:T(8,128)(2,1)S(1)}, bf16[2,128,64]{1,2,0:T(8,128)(2,1)S(1)}, u32[]{:S(2)}, u32[]{:S(2)}) collective-permute-start(bf16[2,128,64]{1,2,0:T(8,128)(2,1)S(1)} %pad_maximum_fusion.3), channel_id=1, source_target_pairs={{0,8},{8,16},{16,24},{24,32},{32,40},{40,48},{48,56},{56,64},{64,7... | collective-permute-start | bytes 98312 | tf_op jit(solution)/shard_map/ppermute | solution.py:36
  164.4 1.2 collective-permute-done.6
  166.5 18.5 %collective-permute-done.5 = bf16[32,2,128,128]{3,2,1,0:T(8,128)(2,1)} collective-permute-done((bf16[32,2,128,128]{3,2,1,0:T(8,128)(2,1)}, bf16[32,2,128,128]{3,2,1,0:T(8,128)(2,1)}, u32[]{:S(2)}, u32[]{:S(2)}) %collective-permute-start.5) | collective-permute-done | bytes 2097184 | tf_op jit(solution)/shard_map/ppermute | solution.py:36
  184.9 3.2 constant_dynamic-update-slice_fusion.17
  188.1 1.1 constant_dynamic-update-slice_fusion.16
  192.6 6.7 %copy.43 = bf16[8,2,8,128,128]{3,2,4,1,0:T(8,128)(2,1)} copy(bf16[8,2,8,128,128]{4,3,1,2,0:T(8,128)(2,1)} %bitcast.6) | data formatting | bytes 8388608 | tf_op jit(solution)/shard_map/transpose | solution.py:127
  199.4 7.3 %reshape.312 = bf16[8,2,1024,128]{2,3,1,0:T(8,128)(2,1)} reshape(bf16[8,2,8,128,128]{3,2,4,1,0:T(8,128)(2,1)} %copy.43) | data formatting | bytes 8388608 | tf_op jit(solution)/shard_map/reshape | solution.py:127
  206.7 71.4 %while.17 = (s32[]{:T(128)}, f32[2,128,64]{1,2,0:T(8,128)S(1)}, f32[2,128]{1,0:T(2,128)S(1)}, s32[8]{0:T(128)S(1)}, bf16[8,2,1024,128]{2,3,1,0:T(8,128)(2,1)}, /...) while((s32[]{:T(128)}, f32[2,128,64]{1,2,0:T(8,128)S(1)}, ...), condition=%wide.region_5.6_spmd.clone, body=%wide.region_1.5_spmd.clone.sunk | while | flops 109366400 | bytes 13740244 | solution.py:141
  208.9 1.1 constant_dynamic-slice_fusion.3
  210.0 1.0 fusion.79
  211.0 2.5 fusion.80
  213.9 1.5 fusion.82
  217.8 1.1 constant_dynamic-slice_fusion.3
  218.9 1.0 fusion.79
  219.9 2.5 fusion.80
  222.8 1.5 fusion.82
  226.7 1.1 constant_dynamic-slice_fusion.3
  227.8 1.0 fusion.79
  228.8 2.5 fusion.80
  231.7 1.5 fusion.82
  235.7 1.1 constant_dynamic-slice_fusion.3
  236.7 1.0 fusion.79
  237.7 2.5 fusion.80
  240.6 1.5 fusion.82
  244.6 1.1 constant_dynamic-slice_fusion.3
  245.7 1.0 fusion.79
  246.7 2.5 fusion.80
  249.6 1.5 fusion.82
  253.5 1.1 constant_dynamic-slice_fusion.3
  254.6 1.0 fusion.79
  255.6 2.5 fusion.80
  258.5 1.5 fusion.82
  262.4 1.1 constant_dynamic-slice_fusion.3
  263.5 1.0 fusion.79
  264.5 2.5 fusion.80
  267.4 1.5 fusion.82
  271.4 1.1 constant_dynamic-slice_fusion.3
  272.5 1.0 fusion.79
  273.4 2.5 fusion.80
  276.3 1.5 fusion.82
  278.2 7.7 %all_to_all.12 = f32[8,1,256]{2,1,0:T(1,128)S(1)} all-to-all(f32[8,1,256]{2,1,0:T(1,128)S(1)} %broadcast_in_dim.81), channel_id=1, replica_groups=mesh['sp'=64,'tp'=8] {'tp'}, dimensions={0} | all-to-all | bytes 16384 | tf_op jit(solution)/shard_map/all_to_all | solution.py:24
  286.3 2.2 fusion.17
  288.5 163.2 %reduce-scatter.2.cloned.1.call-done = bf16[16,2048]{1,0:T(8,128)(2,1)} async-done(((bf16[128,2048]{1,0:T(8,128)(2,1)}), bf16[16,2048]{1,0:T(8,128)(2,1)}) %reduce-scatter.2.cloned.1.call-update) | async-done | bytes 65552 | tf_op jit(solution)/shard_map/reduce_scatter | solution.py:190
  451.7 1.0 fusion.28
  452.7 1.6 fusion.30
  (165 shorter events, 34.3 us)
Async XLA Ops:
  6.5 279.5 %copy-start = (bf16[128,2048]{1,0:T(8,128)(2,1)S(1)}, bf16[128,2048]{1,0:T(8,128)(2,1)}, u32[]{:S(2)}) copy-start(bf16[128,2048]{1,0:T(8,128)(2,1)} %param.29) | copy-start | bytes 1572868
  6.5 18.3 %copy-start.1 = (bf16[2048,128]{1,0:T(8,128)(2,1)S(1)}, bf16[2048,128]{1,0:T(8,128)(2,1)}, u32[]{:S(2)}) copy-start(bf16[2048,128]{1,0:T(8,128)(2,1)} %param.20) | copy-start | bytes 1572868
  6.5 445.2 %reduce-scatter.2.cloned.1.call-start = ((), (), s32[]{:S(2)}) async-start(), calls=%async_computation.3 | async-start | bytes 589824 | tf_op jit(solution)/shard_map/reduce_scatter | solution.py:190
  22.1 57.4 %copy-start.3 = (bf16[2048,64]{0,1:T(8,128)(2,1)S(1)}, bf16[2048,64]{0,1:T(8,128)(2,1)}, u32[]{:S(2)}) copy-start(bf16[2048,64]{0,1:T(8,128)(2,1)} %param.23) | copy-start | bytes 786436
  25.2 7.6 %collective-permute-start = (bf16[1,2,128,128]{3,2,1,0:T(8,128)(2,1)S(1)}, bf16[1,2,128,128]{3,2,1,0:T(8,128)(2,1)S(1)}, u32[]{:S(2)}, u32[]{:S(2)}) collective-permute-start(bf16[1,2,128,128]{3,2,1,0:T(8,128)(2,1)S(1)} %maximum_bitcast_fusion), channel_id=1, source_target_pairs={{0,8},{8,16},{16,24},{24,32},{32,40},{40,48},{48,56},{56,64},{64,7... | collective-permute-start | bytes 196616 | tf_op jit(solution)/shard_map/ppermute | solution.py:36
  32.9 6.0 %collective-permute-start.1 = (bf16[2,2,128,128]{3,2,1,0:T(8,128)(2,1)S(1)}, bf16[2,2,128,128]{3,2,1,0:T(8,128)(2,1)S(1)}, u32[]{:S(2)}, u32[]{:S(2)}) collective-permute-start(bf16[2,2,128,128]{3,2,1,0:T(8,128)(2,1)S(1)} %pad_maximum_fusion.2), channel_id=1, source_target_pairs={{0,16},{8,24},{16,32},{24,40},{32,48},{40,56},{48,64},{56,72},{64,... | collective-permute-start | bytes 393224 | tf_op jit(solution)/shard_map/ppermute | solution.py:36
  38.9 15.5 %collective-permute-start.2 = (bf16[4,2,128,128]{3,2,1,0:T(8,128)(2,1)S(1)}, bf16[4,2,128,128]{3,2,1,0:T(8,128)(2,1)S(1)}, u32[]{:S(2)}, u32[]{:S(2)}) collective-permute-start(bf16[4,2,128,128]{3,2,1,0:T(8,128)(2,1)S(1)} %pad_maximum_fusion.1), channel_id=1, source_target_pairs={{0,32},{8,40},{16,48},{24,56},{32,64},{40,72},{48,80},{56,88},{64,... | collective-permute-start | bytes 786440 | tf_op jit(solution)/shard_map/ppermute | solution.py:36
  54.4 15.2 %collective-permute-start.3 = (bf16[8,2,128,128]{3,2,1,0:T(8,128)(2,1)S(1)}, bf16[8,2,128,128]{3,2,1,0:T(8,128)(2,1)S(1)}, u32[]{:S(2)}, u32[]{:S(2)}) collective-permute-start(bf16[8,2,128,128]{3,2,1,0:T(8,128)(2,1)S(1)} %pad_maximum_fusion), channel_id=1, source_target_pairs={{0,64},{8,72},{16,80},{24,88},{32,96},{40,104},{48,112},{56,120},{... | collective-permute-start | bytes 1572872 | tf_op jit(solution)/shard_map/ppermute | solution.py:36
  73.1 24.4 %collective-permute-start.4 = (bf16[16,2,128,128]{3,2,1,0:T(8,128)(2,1)}, bf16[16,2,128,128]{3,2,1,0:T(8,128)(2,1)S(1)}, u32[]{:S(2)}, u32[]{:S(2)}) collective-permute-start(bf16[16,2,128,128]{3,2,1,0:T(8,128)(2,1)} %constant_dynamic-update-slice_fusion), channel_id=1, source_target_pairs={{0,128},{8,136},{16,144},{24,152},{32,160},{40,168},{48,176},{56,1... | collective-permute-start | bytes 3145736 | tf_op jit(solution)/shard_map/ppermute | solution.py:36
  79.4 84.7 %copy-start.2 = (bf16[2048,128]{1,0:T(8,128)(2,1)S(1)}, bf16[2048,128]{1,0:T(8,128)(2,1)}, u32[]{:S(2)}) copy-start(bf16[2048,128]{1,0:T(8,128)(2,1)} %param.19) | copy-start | bytes 1572868
  79.7 86.3 %copy-start.5 = (f32[2]{0:T(128)S(1)}, f32[2]{0:T(128)}, u32[]{:S(2)}) copy-start(f32[2]{0:T(128)} %param.26) | copy-start | bytes 28
  102.0 82.9 %collective-permute-start.5 = (bf16[32,2,128,128]{3,2,1,0:T(8,128)(2,1)}, bf16[32,2,128,128]{3,2,1,0:T(8,128)(2,1)}, u32[]{:S(2)}, u32[]{:S(2)}) collective-permute-start(bf16[32,2,128,128]{3,2,1,0:T(8,128)(2,1)} %constant_dynamic-update-slice_fusion.5), channel_id=1, source_target_pairs={{0,256},{8,264},{16,272},{24,280},{32,288},{40,296},{48,304},{56,3... | collective-permute-start | bytes 6291464 | tf_op jit(solution)/shard_map/ppermute | solution.py:36
  144.9 20.7 %collective-permute-start.6 = (bf16[2,128,64]{1,2,0:T(8,128)(2,1)S(1)}, bf16[2,128,64]{1,2,0:T(8,128)(2,1)S(1)}, u32[]{:S(2)}, u32[]{:S(2)}) collective-permute-start(bf16[2,128,64]{1,2,0:T(8,128)(2,1)S(1)} %pad_maximum_fusion.3), channel_id=1, source_target_pairs={{0,8},{8,16},{16,24},{24,32},{32,40},{40,48},{48,56},{56,64},{64,7... | collective-permute-start | bytes 98312 | tf_op jit(solution)/shard_map/ppermute | solution.py:36
  199.4 7.3 %copy-start.8 = (f32[2]{0:T(128)S(1)}, f32[2]{0:T(128)}, u32[]{:S(2)}) copy-start(f32[2]{0:T(128)} %param.25) | copy-start | bytes 28
  206.7 79.2 %copy-start.6 = (f32[128]{0:T(128)S(1)}, f32[128]{0:T(128)}, u32[]{:S(2)}) copy-start(f32[128]{0:T(128)} %param.28) | copy-start | bytes 1540
  206.7 79.2 %copy-start.7 = (f32[128]{0:T(128)S(1)}, f32[128]{0:T(128)}, u32[]{:S(2)}) copy-start(f32[128]{0:T(128)} %param.27) | copy-start | bytes 1540
  278.1 174.6 %copy-start.4 = (f32[2048]{0:T(1024)S(1)}, f32[2048]{0:T(1024)}, u32[]{:S(2)}) copy-start(f32[2048]{0:T(1024)} %param.31) | copy-start | bytes 24580
Sparse Core Ops, SparseCore 0:
  288.6 163.0 reduce-scatter.1
where the time goes:
time: 462 us; the launch traced here: 461 us
  waiting for transfers between devices  217 us (47%)
  starting transfers between devices  93.6 us (20%)
  other arithmetic  52.3 us (11%)
  local copies, waits for them, and re-layouts  44.2 us (10%)
  blocking collectives  22.1 us (5%)
  matrix products  17.5 us (4%)
  between operations  13.7 us (3%)
    reduce_scatter x1, waiting for transfers between devices, shards(): lax.psum_scatter((total + jnp.dot(window_normed, w_out_window, preferred_...  163 us
    ppermute x7, starting transfers between devices, passed_along(): lax.ppermute(value, axis, [(source, source + steps) for source in range(i...  93.6 us
    ppermute x7, waiting for transfers between devices, passed_along(): lax.ppermute(value, axis, [(source, source + steps) for source in range(i...  53.7 us
    all_to_all x2, blocking collectives, from_everyone(): lax.all_to_all(jnp.broadcast_to(array[None], (size, *array.shape)), axis,...  22.1 us
    another operation x16, other arithmetic  20.6 us
    unnamed x35, local copies, waits for them, and re-layouts  14.9 us
    convert_element_type x8, other arithmetic, stick_block(): stick_weights = stick_weights.astype(jnp.bfloat16)  12 us
  transfers between devices with their start and end apart: 8, of which 8 were waited for; matrix products, arithmetic and copies ran while one was open for 1% of the time, Pallas kernels for 0%

commit v1 on v0

v1 whole, which is shorter than its diff:
```python
import functools

import jax
import jax.numpy as jnp
from jax import lax
from jax.experimental import pallas as pl
from jax.experimental.pallas import tpu as pltpu
from jax.sharding import PartitionSpec as P

T = 128
D = 2048
CH = 256
NY = 8
NZ = 8
NTP = 8
NX = 4
LOG2E = 1.4426950408889634
EPS = 1e-06
PACK = D + 128
PROWS = T + 16
MESH = pl.DeviceIdType.MESH
F32 = jnp.float32
BF16 = jnp.bfloat16


def dot(a, b):
    return jnp.dot(a, b, preferred_element_type=F32)


def dot_nt(a, b):
    return lax.dot_general(a, b, (((1,), (1,)), ((), ())), preferred_element_type=F32)


def iota(shape, dim):
    return lax.broadcasted_iota(jnp.int32, shape, dim)


def with_squares(ref, out):
    total = jnp.sum(out * out, axis=1, keepdims=True)
    high = total.astype(BF16).astype(F32)
    lane = iota((T, 128), 1)
    ref[:, D:] = jnp.where(lane == 0, high, jnp.where(lane == 1, total - high, 0.0)).astype(BF16)


def kernel(
    tok, pre, wqs, wks, wvs, wqw, wkw, wvw, bias, sinks, sgain, wgain, wos, wow, post,
    out,
    tok_all, w4, wk6, wv6, wo_s, wo_w, pre_v, sg_v, wg_v, post_v,
    acc4, acck, accv, sq, kvb, qb, kbd, vbd, tri, ones,
    wkv, pwkv, pout, prec, acc_p, acc_l, ab, bb, ra, rb,
    lsem, s_a, r_a, s_k, r_k, r_k4, s_q, r_q, s_w, r_w, s_p, r_p, s_ra, r_ra, s_rb, r_rb,
):
    sp = lax.axis_index("sp")
    tp = lax.axis_index("tp")
    z = sp // NY
    y = sp % NY
    x = tp // 2
    c = tp % 2

    def rcopy(src, dst, ssem, rsem, dev):
        return pltpu.make_async_remote_copy(
            src_ref=src, dst_ref=dst, send_sem=ssem, recv_sem=rsem, device_id=dev, device_id_type=MESH
        )

    loads = [pltpu.make_async_copy(tok, tok_all.at[tp], lsem.at[0])]
    pairs = [
        (pre, pre_v), (wks, w4.at[:, pl.ds(0, 128)]), (wvs, w4.at[:, pl.ds(128, 128)]),
        (wqs, w4.at[:, pl.ds(256, 128)]), (wqw, w4.at[:, pl.ds(384, 128)]), (wkw, wk6), (wvw, wv6),
        (sgain, sg_v), (wgain, wg_v), (post, post_v), (wos, wo_s), (wow, wo_w),
    ]
    for n, (src, dst) in enumerate(pairs):
        loads.append(pltpu.make_async_copy(src, dst, lsem.at[n + 1]))
    for load in loads:
        load.start()

    barrier = pltpu.get_barrier_semaphore()
    greeted = [(sp, (tp + d) % NTP) for d in range(1, NTP)]
    greeted += [(z * NY + (y + d) % NY, tp) for d in (1, 2, NY - 2, NY - 1)]
    greeted += [(((z + d) % NZ) * NY + y, tp) for d in range(1, NZ)]
    greeted += [((sp + d) % (NY * NZ), tp) for d in (1, NY * NZ - 1)]
    for dev in greeted:
        pl.semaphore_signal(barrier, inc=1, device_id=dev, device_id_type=MESH)

    row2, col2 = iota((256, 256), 0), iota((256, 256), 1)
    tri[...] = jnp.where((row2 > col2) & (row2 // T == col2 // T), 1.0, 0.0).astype(BF16)
    ones[...] = jnp.where(iota((256, 128), 0) // T == iota((256, 128), 1) // 64, 1.0, 0.0).astype(BF16)
    acc4[...] = jnp.zeros_like(acc4)
    acck[...] = jnp.zeros_like(acck)
    accv[...] = jnp.zeros_like(accv)
    sq[...] = jnp.zeros_like(sq)

    pl.semaphore_wait(barrier, len(greeted))
    loads[0].wait()

    partner = x * 2 + (1 - c)
    own_tok = tok_all.at[tp]
    tok_sends = []
    for n, d in enumerate((2, 1, 3)):
        peer = ((x + d) % NX) * 2 + c
        tok_sends.append(rcopy(own_tok, own_tok, s_a.at[n], r_a.at[tp], (sp, peer)))
    tok_sends.append(rcopy(own_tok, own_tok, s_a.at[3], r_a.at[tp], (sp, partner)))
    for send in tok_sends:
        send.start()
    for load in loads[1:8]:
        load.wait()

    def feature_step(i, _):
        dist = jnp.where(i < 2, 0, jnp.where((i == 2) | (i == 5), 1, jnp.where((i == 3) | (i == 6), 3, 2)))
        core = jnp.where((i == 1) | (i >= 5), 1 - c, c)
        src = ((x + dist) % NX) * 2 + core
        block = tok_all.at[src]

        @pl.when(i > 0)
        def _():
            rcopy(block, block, s_a.at[0], r_a.at[src], (sp, partner)).wait_recv()

        @pl.when((i >= 2) & (i <= 4))
        def _():
            rcopy(block, block, s_a.at[i + 2], r_a.at[src], (sp, partner)).start()

        feats = block[...].astype(F32)
        sq[...] += feats[:, :128] * feats[:, :128] + feats[:, 128:] * feats[:, 128:]
        at = pl.ds(pl.multiple_of(src * CH, CH), CH)
        scaled = (feats * pre_v[:, at]).astype(BF16)
        acc4[...] += dot(scaled, w4[at, :])
        acck[...] += dot(scaled, wk6[at, :])
        accv[...] += dot(scaled, wv6[at, :])
        return 0

    lax.fori_loop(0, NTP, feature_step, 0)
    inv = lax.rsqrt(jnp.sum(sq[...], axis=1, keepdims=True) * (1.0 / D) + EPS)

    kvb[y, 0] = (acc4[:, 0:128] * inv).T.astype(BF16)
    kvb[y, 1] = (acc4[:, 128:256] * inv).astype(BF16)
    own_kv = kvb.at[y]
    kv_sends = []
    for n, d in enumerate((2, NY - 2, 1, NY - 1)):
        kv_sends.append(rcopy(own_kv, own_kv, s_k.at[n], r_k.at[y], (z * NY + (y + d) % NY, tp)))
    for send in kv_sends:
        send.start()
    qb[z] = (acc4[:, 256:384] * (inv * (0.125 * LOG2E))).astype(BF16)

    def q_send(i):
        return rcopy(qb.at[z], qb.at[z], s_q.at[i], r_q.at[z], (i * NY + y, tp))

    def q_start(i, _):
        q_send(i).start()
        return 0

    lax.fori_loop(0, z, q_start, 0)
    own_k = (acck[...] * inv).astype(BF16)
    own_v = (accv[...] * inv).astype(BF16)
    wkv[...] = jnp.concatenate([own_k, own_v], axis=1)
    win_send = rcopy(wkv, pwkv, s_w, r_w, ((sp + 1) % (NY * NZ), tp))
    win_send.start()

    query_w = (acc4[:, 384:512] * inv).astype(BF16)
    for load in loads[8:]:
        load.wait()
    rcopy(wkv, pwkv, s_w, r_w, ((sp + NY * NZ - 1) % (NY * NZ), tp)).wait_recv()
    prev = pwkv[...]
    keys = jnp.concatenate([prev[:, :64], own_k], axis=0)
    values = jnp.concatenate([prev[:, 64:], own_v], axis=0)
    q_row, k_col = iota((T, 2 * T), 0), iota((T, 2 * T), 1)
    usable = (k_col > q_row) & (k_col <= q_row + T) & ((k_col >= T) | (sp > 0))
    outs = []
    for h in range(2):
        logit = dot_nt(query_w[:, 64 * h : 64 * h + 64], keys) * (0.125 * LOG2E)
        logit = jnp.where(usable, logit, -jnp.inf)
        sink = sinks[h] * LOG2E
        top = jnp.maximum(jnp.max(logit, axis=1, keepdims=True), sink)
        weight = jnp.exp2(logit - top)
        norm = jnp.sum(weight, axis=1, keepdims=True) + jnp.exp2(sink - top)
        outs.append(dot((weight / norm).astype(BF16), values))
    win_out = jnp.concatenate(outs, axis=1).astype(BF16).astype(F32)
    with_squares(bb, win_out)
    scaled_w = (win_out * wg_v[...]).astype(BF16)
    for n in range(4):
        bb[:, n * 512 : n * 512 + 512] = dot(scaled_w, wo_w[:, n * 512 : n * 512 + 512]).astype(BF16)

    def scatter(buf, dst, ssem, rsem):
        sends = []
        for d in (4, 5, 3, 2, 6, 7, 1):
            to = (tp + d) % NTP
            rows = buf.at[pl.ds(pl.multiple_of(to * 16, 16), 16), :]
            sends.append(rcopy(rows, dst.at[tp], ssem.at[d], rsem.at[tp], (sp, to)))
        for send in sends:
            send.start()
        return sends

    win_sends = scatter(bb, rb, s_rb, r_rb)

    before, after = (y + NY - 2) % NY, (y + 2) % NY
    row_of = lambda d: (z * NY + (y + d) % NY, tp)
    relays = [
        (before, [(kvb.at[before], 1, r_k.at[before]), (kvb.at[before, 0], 2, r_k4.at[0])]),
        (after, [(kvb.at[after], NY - 1, r_k.at[after]), (kvb.at[after, 1], NY - 2, r_k4.at[1])]),
    ]
    for side, (src, copies) in enumerate(relays):
        rcopy(kvb.at[src], kvb.at[src], s_k.at[0], r_k.at[src], row_of(1)).wait_recv()
        for n, (ref, d, rsem) in enumerate(copies):
            send = rcopy(ref, ref, s_k.at[4 + 2 * side + n], rsem, row_of(d))
            send.start()
            kv_sends.append(send)
    for d in (1, 7, 3, 5):
        src = (y + d) % NY
        rcopy(kvb.at[src], kvb.at[src], s_k.at[0], r_k.at[src], row_of(1)).wait_recv()
    far = (y + 4) % NY
    for n in range(2):
        rcopy(kvb.at[far, n], kvb.at[far, n], s_k.at[0], r_k4.at[n], row_of(1)).wait_recv()

    def spread(j, _):
        key_t, val = kvb[j, 0], kvb[j, 1]
        zero = jnp.zeros_like(key_t)
        feat = iota((T, 128), 0) < 64
        kbd[j, :, :T] = jnp.where(feat, key_t, zero)
        kbd[j, :, T:] = jnp.where(feat, zero, key_t)
        lane = iota((T, 128), 1) < 64
        vbd[j, :T, :] = jnp.where(lane, val, zero)
        vbd[j, T:, :] = jnp.where(lane, zero, val)
        return 0

    lax.fori_loop(0, NY, spread, 0)

    bias_row = jnp.where(iota((1, 2 * T), 1) < T, bias[0] * LOG2E, bias[1] * LOG2E)

    def tile(q, j, usable):
        score = dot(q, kbd[j]) + bias_row
        soft = jnp.maximum(score, jnp.log(1.0 + jnp.exp2(jnp.minimum(score, 126.0))) * LOG2E)
        if usable is not None:
            soft = jnp.where(usable, soft, 0.0)
        soft_b = soft.astype(BF16)
        weight = jnp.exp2((score - soft) - dot(soft_b, tri[...]))
        if usable is not None:
            weight = jnp.where(usable, weight, 0.0)
        return dot(weight.astype(BF16), vbd[j]), dot(soft_b, ones[...])

    def log_rows(total):
        flipped = total.T
        return flipped[0:1, :], flipped[64:65, :]

    def p_send(to):
        return rcopy(pout.at[to], prec.at[z], s_p.at[to], r_p.at[z], (to * NY + y, tp))

    def query_step(i, _):
        zq = NZ - 1 - i
        rcopy(qb.at[zq], qb.at[zq], s_q.at[0], r_q.at[zq], (zq * NY + y, tp)).wait_recv()
        q = qb[zq]
        part, logs = tile(q, NY - 1, None)
        for j in range(NY - 2, -1, -1):
            p_j, l_j = tile(q, j, None)
            part = part + jnp.exp2(-logs) * p_j
            logs = logs + l_j
        pout[zq, :T, :] = part.astype(BF16)
        l0, l1 = log_rows(logs)
        h0, h1 = l0.astype(BF16).astype(F32), l1.astype(BF16).astype(F32)
        row = iota((16, 128), 0)
        packed = jnp.where(row == 0, h0, jnp.where(row == 1, l0 - h0, jnp.where(row == 2, h1, l1 - h1)))
        pout[zq, T:, :] = packed.astype(BF16)
        p_send(zq).start()
        return 0

    lax.fori_loop(0, NZ - 1 - z, query_step, 0)

    acc_p[...] = jnp.zeros_like(acc_p)
    acc_l[...] = jnp.zeros_like(acc_l)
    own_q = qb[z]

    def own_step(i, _):
        j = NY - 1 - i
        usable = (j * T + k_col % T) < (y * T + q_row)
        p_j, l_j = tile(own_q, j, usable)
        acc_p[...] += jnp.exp2(-acc_l[...]) * p_j
        acc_l[...] += l_j
        return 0

    lax.fori_loop(NY - 1 - y, NY, own_step, 0)

    def merge(i, logs):
        l0, l1 = logs
        src = z - 1 - i
        rcopy(pout.at[src], prec.at[src], s_p.at[0], r_p.at[src], (src * NY + y, tp)).wait_recv()
        factor = jnp.concatenate(
            [jnp.broadcast_to(jnp.exp2(-l0), (64, 128)), jnp.broadcast_to(jnp.exp2(-l1), (64, 128))], axis=0
        ).T
        acc_p[...] += factor * prec[src, :T, :].astype(F32)
        more = prec[src, T:, :].astype(F32)
        return l0 + (more[0:1] + more[1:2]), l1 + (more[2:3] + more[3:4])

    lax.fori_loop(0, z, merge, log_rows(acc_l[...]))

    stick_out = acc_p[...].astype(BF16).astype(F32)
    with_squares(ab, stick_out)
    scaled_s = (stick_out * sg_v[...]).astype(BF16)
    for n in range(4):
        ab[:, n * 512 : n * 512 + 512] = dot(scaled_s, wo_s[:, n * 512 : n * 512 + 512]).astype(BF16)
    stick_sends = scatter(ab, ra, s_ra, r_ra)

    def gathered(buf, dst, rsem):
        mine = pl.ds(pl.multiple_of(tp * 16, 16), 16)
        total = buf[mine, :].astype(F32)
        for d in (1, 2, 6, 7, 3, 5, 4):
            src = (tp + d) % NTP
            rcopy(dst.at[src], dst.at[src], s_ra.at[0], rsem.at[src], (sp, src)).wait_recv()
            total = total + dst[src].astype(F32)
        scale = lax.rsqrt(jnp.sum(total[:, D:], axis=1, keepdims=True) * (1.0 / 1024) + EPS)
        return total[:, :D] * scale

    combined = gathered(bb, rb, r_rb)
    combined = combined + gathered(ab, ra, r_ra)
    mean = jnp.sum(combined * combined, axis=1, keepdims=True) * (1.0 / D)
    out[...] = (combined * lax.rsqrt(mean + EPS) * post_v[...]).astype(BF16)

    for send in tok_sends + kv_sends + [win_send] + win_sends + stick_sends:
        send.wait_send()
    for n in (4, 5, 6):
        rcopy(own_tok, own_tok, s_a.at[n], r_a.at[tp], (sp, partner)).wait_send()

    def q_drain(i, _):
        q_send(i).wait_send()
        return 0

    lax.fori_loop(0, z, q_drain, 0)

    def p_drain(i, _):
        p_send(NZ - 1 - i).wait_send()
        return 0

    lax.fori_loop(0, NZ - 1 - z, p_drain, 0)


def shards(
    tokens, pre_gain, w_query_stick, w_key_stick, w_value_stick, w_query_window, w_key_window, w_value_window,
    stick_bias, sinks, stick_gain, window_gain, w_out_stick, w_out_window, post_gain,
):
    anywhere = pl.BlockSpec(memory_space=pl.ANY)
    scalars = pl.BlockSpec(memory_space=pltpu.SMEM)
    dma = pltpu.SemaphoreType.DMA
    vm = pltpu.VMEM
    scratch = [
        vm((NTP, T, CH), BF16), vm((D, 512), BF16), vm((D, 64), BF16), vm((D, 64), BF16),
        vm((128, D), BF16), vm((128, D), BF16), vm((1, D), F32), vm((1, 128), F32), vm((1, 128), F32), vm((1, D), F32),
        vm((T, 512), F32), vm((T, 64), F32), vm((T, 64), F32), vm((T, 128), F32),
        vm((NY, 2, T, 128), BF16), vm((NZ, T, 128), BF16), vm((NY, 128, 2 * T), BF16), vm((NY, 2 * T, 128), BF16),
        vm((256, 256), BF16), vm((256, 128), BF16),
        vm((T, 128), BF16), vm((T, 128), BF16), vm((NZ, PROWS, 128), BF16), vm((NZ, PROWS, 128), BF16),
        vm((T, 128), F32), vm((T, 128), F32), vm((T, PACK), BF16), vm((T, PACK), BF16),
        vm((NTP, 16, PACK), BF16), vm((NTP, 16, PACK), BF16),
        dma((13,)), dma((7,)), dma((NTP,)), dma((8,)), dma((NY,)), dma((2,)), dma((NZ,)), dma((NZ,)), dma, dma,
        dma((NZ,)), dma((NZ,)), dma((NTP,)), dma((NTP,)), dma((NTP,)), dma((NTP,)),
    ]
    return pl.pallas_call(
        kernel,
        out_shape=jax.ShapeDtypeStruct((T // NTP, D), BF16),
        in_specs=[anywhere] * 8 + [scalars] * 2 + [anywhere] * 5,
        out_specs=pl.BlockSpec(memory_space=pltpu.VMEM),
        scratch_shapes=scratch,
        compiler_params=pltpu.CompilerParams(
            collective_id=0, has_side_effects=True, vmem_limit_bytes=48 * 1024 * 1024
        ),
    )(
        tokens, pre_gain.reshape(1, -1), w_query_stick, w_key_stick, w_value_stick, w_query_window,
        w_key_window, w_value_window, stick_bias, sinks, stick_gain.reshape(1, -1), window_gain.reshape(1, -1),
        w_out_stick, w_out_window, post_gain.reshape(1, -1),
    )


def solution(mesh):
    in_specs = (
        P("sp", "tp"),
        P(),
        P(None, "tp"),
        P(None, "tp"),
        P(None, "tp"),
        P(None, "tp"),
        P(None, "tp"),
        P(None, "tp"),
        P("tp"),
        P("tp"),
        P("tp"),
        P("tp"),
        P("tp", None),
        P("tp", None),
        P(),
    )
    out_specs = P(("sp", "tp"), None)
    return jax.shard_map(shards, mesh=mesh, in_specs=in_specs, out_specs=out_specs, check_vma=False)
```

time: 462 us -> 75.8 us (0.16)
  the two profiles are of different devices: /device:TPU:8 before, /device:TPU:48 now
where the time goes in v1:
time: 75.8 us; the launch traced here: 75.4 us
  Pallas kernels  64.1 us (85%)
  local copies, waits for them, and re-layouts  11.2 us (15%)
    pallas_call x1, Pallas kernels, shards(): pl.pallas_call(kernel, out_shape=jax.ShapeDtypeStruct((T // NTP, D), BF16...  64.1 us
    unnamed x29, local copies, waits for them, and re-layouts  11.2 us

profile of v1, /device:TPU:48, one launch (start us, length us, event | category | flops | bytes accessed | tf_op | source)
XLA Modules:
  0.0 75.4 jit_solution(18368648360020284984)
XLA Ops:
  0.0 0.0 copy-start.1
  0.0 0.0 copy-start.2
  0.0 1.3 %copy.16.wkw = bf16[2048,64]{1,0:T(8,128)(2,1)S(1)} copy(bf16[2048,64]{0,1:T(8,128)(2,1)} %param.21) | data formatting | bytes 524288 | tf_op args[6]
  1.3 0.0 copy-start
  1.3 1.3 %copy.17.wvw = bf16[2048,64]{1,0:T(8,128)(2,1)S(1)} copy(bf16[2048,64]{0,1:T(8,128)(2,1)} %param.22) | data formatting | bytes 524288 | tf_op args[7]
  2.6 0.0 copy-done.1
  2.6 0.0 copy-done.2
  2.6 0.0 copy-done
  2.6 0.0 copy-start.3
  2.7 1.0 %copy-done.3 = bf16[2048,128]{1,0:T(8,128)(2,1)S(1)} copy-done((bf16[2048,128]{1,0:T(8,128)(2,1)S(1)}, bf16[2048,128]{1,0:T(8,128)(2,1)}, u32[]{:S(2)}) %copy-start.3) | copy-done | bytes 524312
  3.7 0.0 copy-start.4
  3.7 1.0 %copy-done.4 = bf16[128,2048]{1,0:T(8,128)(2,1)S(1)} copy-done((bf16[128,2048]{1,0:T(8,128)(2,1)S(1)}, bf16[128,2048]{1,0:T(8,128)(2,1)}, u32[]{:S(2)}) %copy-start.4) | copy-done | bytes 524312
  4.7 0.0 copy-start.5
  4.7 1.0 %copy-done.5 = bf16[128,2048]{1,0:T(8,128)(2,1)S(1)} copy-done((bf16[128,2048]{1,0:T(8,128)(2,1)S(1)}, bf16[128,2048]{1,0:T(8,128)(2,1)}, u32[]{:S(2)}) %copy-start.5) | copy-done | bytes 524312
  5.8 0.0 copy-start.6
  5.8 0.8 %copy-done.6 = bf16[128,256]{1,0:T(8,128)(2,1)S(1)} copy-done((bf16[128,256]{1,0:T(8,128)(2,1)S(1)}, bf16[128,256]{1,0:T(8,128)(2,1)}, u32[]{:S(2)}) %copy-start.6) | copy-done | bytes 65560
  6.6 0.0 copy-start.7
  6.6 0.7 copy-done.7
  7.3 0.0 copy-start.8
  7.3 0.7 copy-done.8
  8.0 0.0 copy-start.9
  8.0 0.7 copy-done.9
  8.7 0.0 copy-start.10
  8.7 0.7 copy-done.10
  9.3 0.0 copy-start.11
  9.3 0.7 copy-done.11
  10.0 0.0 copy-start.12
  10.0 0.7 copy-done.12
  10.6 64.1 %shard_map.145 = bf16[16,2048]{1,0:T(8,128)(2,1)S(1)} custom-call(bf16[128,256]{1,0:T(8,128)(2,1)S(1)} %copy-done.6, f32[1,2048]{1,0:T(1,128)S(1)} %bitcast.4, bf16[2048,128]{1,0:T(8,128)(2,1)S(1)} %copy-done, bf16[2048,128]{1,0:T(8,128)(2,1)S(1)} %copy-done.1, bf16[2048,128]{1,0:T(8,128)(2,1)S(1)} %copy-done.2, bf16[2048,128]{1,0:T(8,128)(2,1)S(1)} %copy-done.3, ...), custom_call_target="tpu_custom_call" | custom-call | tf_op jit(solution)/shard_map/pallas_call | solution.py:352
  74.7 0.6 copy.19
Async XLA Ops:
  0.0 2.6 %copy-start.1 = (bf16[2048,128]{1,0:T(8,128)(2,1)S(1)}, bf16[2048,128]{1,0:T(8,128)(2,1)}, u32[]{:S(2)}) copy-start(bf16[2048,128]{1,0:T(8,128)(2,1)} %wks.1) | copy-start | bytes 1572868
  0.0 2.6 %copy-start.2 = (bf16[2048,128]{1,0:T(8,128)(2,1)S(1)}, bf16[2048,128]{1,0:T(8,128)(2,1)}, u32[]{:S(2)}) copy-start(bf16[2048,128]{1,0:T(8,128)(2,1)} %wvs.1) | copy-start | bytes 1572868
  1.3 1.3 %copy-start = (bf16[2048,128]{1,0:T(8,128)(2,1)S(1)}, bf16[2048,128]{1,0:T(8,128)(2,1)}, u32[]{:S(2)}) copy-start(bf16[2048,128]{1,0:T(8,128)(2,1)} %wqs.1) | copy-start | bytes 1572868
  2.6 1.0 %copy-start.3 = (bf16[2048,128]{1,0:T(8,128)(2,1)S(1)}, bf16[2048,128]{1,0:T(8,128)(2,1)}, u32[]{:S(2)}) copy-start(bf16[2048,128]{1,0:T(8,128)(2,1)} %wqw.1) | copy-start | bytes 1572868
  3.7 1.0 %copy-start.4 = (bf16[128,2048]{1,0:T(8,128)(2,1)S(1)}, bf16[128,2048]{1,0:T(8,128)(2,1)}, u32[]{:S(2)}) copy-start(bf16[128,2048]{1,0:T(8,128)(2,1)} %wos.1) | copy-start | bytes 1572868
  4.7 1.0 %copy-start.5 = (bf16[128,2048]{1,0:T(8,128)(2,1)S(1)}, bf16[128,2048]{1,0:T(8,128)(2,1)}, u32[]{:S(2)}) copy-start(bf16[128,2048]{1,0:T(8,128)(2,1)} %wow.1) | copy-start | bytes 1572868
  5.8 0.8 %copy-start.6 = (bf16[128,256]{1,0:T(8,128)(2,1)S(1)}, bf16[128,256]{1,0:T(8,128)(2,1)}, u32[]{:S(2)}) copy-start(bf16[128,256]{1,0:T(8,128)(2,1)} %tok.1) | copy-start | bytes 196612
  6.6 0.7 copy-start.7
  7.3 0.7 copy-start.8
  8.0 0.7 copy-start.9
  8.7 0.7 copy-start.10
  9.3 0.7 copy-start.11
  10.0 0.7 copy-start.12

commit v2 on v1

--- a/solution.py
+++ b/solution.py
@@ -45,10 +45,10 @@
 def kernel(
     tok, pre, wqs, wks, wvs, wqw, wkw, wvw, bias, sinks, sgain, wgain, wos, wow, post,
     out,
-    tok_all, w4, wk6, wv6, wo_s, wo_w, pre_v, sg_v, wg_v, post_v,
-    acc4, acck, accv, sq, kvb, qb, kbd, vbd, tri, ones,
-    wkv, pwkv, pout, prec, acc_p, acc_l, ab, bb, ra, rb,
-    lsem, s_a, r_a, s_k, r_k, r_k4, s_q, r_q, s_w, r_w, s_p, r_p, s_ra, r_ra, s_rb, r_rb,
+    tok_all, w4, w_win, wo_s, wo_w, pre_v, sg_v, wg_v, post_v,
+    acc4, acc_w, sq, kvb, qb, kbd, vbd, tri, soft_b, diff, weight_b, parts, logs,
+    wkv, pwkv, pout, prec, acc_p, ab, bb, ra, rb, bias_s, sinks_s,
+    lsem, s_a, r_a, s_k, r_k, r_k4, s_q, r_q, s_w, r_w, ready, s_p, r_p, s_ra, r_ra, s_rb, r_rb,
 ):
     sp = lax.axis_index("sp")
     tp = lax.axis_index("tp")
@@ -65,8 +65,9 @@
     loads = [pltpu.make_async_copy(tok, tok_all.at[tp], lsem.at[0])]
     pairs = [
         (pre, pre_v), (wks, w4.at[:, pl.ds(0, 128)]), (wvs, w4.at[:, pl.ds(128, 128)]),
-        (wqs, w4.at[:, pl.ds(256, 128)]), (wqw, w4.at[:, pl.ds(384, 128)]), (wkw, wk6), (wvw, wv6),
-        (sgain, sg_v), (wgain, wg_v), (post, post_v), (wos, wo_s), (wow, wo_w),
+        (wqs, w4.at[:, pl.ds(256, 128)]), (wqw, w4.at[:, pl.ds(384, 128)]),
+        (wkw, w_win.at[pl.ds(0, 64), :]), (wvw, w_win.at[pl.ds(64, 64), :]),
+        (bias, bias_s), (sinks, sinks_s), (sgain, sg_v), (wgain, wg_v), (post, post_v), (wos, wo_s), (wow, wo_w),
     ]
     for n, (src, dst) in enumerate(pairs):
         loads.append(pltpu.make_async_copy(src, dst, lsem.at[n + 1]))
@@ -74,22 +75,43 @@
         load.start()
 
     barrier = pltpu.get_barrier_semaphore()
+
+    def greet(dev):
+        pl.semaphore_signal(barrier, inc=1, device_id=dev, device_id_type=MESH)
+
     greeted = [(sp, (tp + d) % NTP) for d in range(1, NTP)]
     greeted += [(z * NY + (y + d) % NY, tp) for d in (1, 2, NY - 2, NY - 1)]
-    greeted += [(((z + d) % NZ) * NY + y, tp) for d in range(1, NZ)]
-    greeted += [((sp + d) % (NY * NZ), tp) for d in (1, NY * NZ - 1)]
     for dev in greeted:
-        pl.semaphore_signal(barrier, inc=1, device_id=dev, device_id_type=MESH)
+        greet(dev)
+
+    def greet_row(i, _):
+        greet((i * NY + y, tp))
+        return 0
+
+    lax.fori_loop(z + 1, NZ, greet_row, 0)
+    has_next = sp < NY * NZ - 1
+    has_prev = sp > 0
+    starts_row = (y == 0) & has_prev
+    ends_row = (y == NY - 1) & has_next
+    nxt = ((sp + 1) % (NY * NZ), tp)
+    before_me = ((sp + NY * NZ - 1) % (NY * NZ), tp)
+
+    @pl.when(ends_row)
+    def _():
+        greet(nxt)
 
     row2, col2 = iota((256, 256), 0), iota((256, 256), 1)
     tri[...] = jnp.where((row2 > col2) & (row2 // T == col2 // T), 1.0, 0.0).astype(BF16)
-    ones[...] = jnp.where(iota((256, 128), 0) // T == iota((256, 128), 1) // 64, 1.0, 0.0).astype(BF16)
     acc4[...] = jnp.zeros_like(acc4)
-    acck[...] = jnp.zeros_like(acck)
-    accv[...] = jnp.zeros_like(accv)
+    acc_w[...] = jnp.zeros_like(acc_w)
     sq[...] = jnp.zeros_like(sq)
 
-    pl.semaphore_wait(barrier, len(greeted))
+    pl.semaphore_wait(barrier, len(greeted) + z + jnp.where(starts_row, 1, 0))
+
+    @pl.when(starts_row)
+    def _():
+        pl.semaphore_signal(ready, inc=1, device_id=before_me, device_id_type=MESH)
+
     loads[0].wait()
 
     partner = x * 2 + (1 - c)
@@ -123,12 +145,24 @@
         at = pl.ds(pl.multiple_of(src * CH, CH), CH)
         scaled = (feats * pre_v[:, at]).astype(BF16)
         acc4[...] += dot(scaled, w4[at, :])
-        acck[...] += dot(scaled, wk6[at, :])
-        accv[...] += dot(scaled, wv6[at, :])
+        acc_w[...] += dot_nt(scaled, w_win[:, at])
         return 0
 
     lax.fori_loop(0, NTP, feature_step, 0)
     inv = lax.rsqrt(jnp.sum(sq[...], axis=1, keepdims=True) * (1.0 / D) + EPS)
+
+    own_pair = (acc_w[...] * inv).astype(BF16)
+    wkv[...] = own_pair
+
+    @pl.when(ends_row)
+    def _():
+        pl.semaphore_wait(ready, 1)
+
+    win_send = rcopy(wkv, pwkv, s_w, r_w, nxt)
+
+    @pl.when(has_next)
+    def _():
+        win_send.start()
 
     kvb[y, 0] = (acc4[:, 0:128] * inv).T.astype(BF16)
     kvb[y, 1] = (acc4[:, 128:256] * inv).astype(BF16)
@@ -148,26 +182,29 @@
         return 0
 
     lax.fori_loop(0, z, q_start, 0)
-    own_k = (acck[...] * inv).astype(BF16)
-    own_v = (accv[...] * inv).astype(BF16)
-    wkv[...] = jnp.concatenate([own_k, own_v], axis=1)
-    win_send = rcopy(wkv, pwkv, s_w, r_w, ((sp + 1) % (NY * NZ), tp))
-    win_send.start()
 
     query_w = (acc4[:, 384:512] * inv).astype(BF16)
     for load in loads[8:]:
         load.wait()
-    rcopy(wkv, pwkv, s_w, r_w, ((sp + NY * NZ - 1) % (NY * NZ), tp)).wait_recv()
+
+    @pl.when(has_prev)
+    def _():
+        rcopy(wkv, pwkv, s_w, r_w, before_me).wait_recv()
+
+    @pl.when(jnp.logical_not(has_prev))
+    def _():
+        pwkv[...] = jnp.zeros_like(pwkv)
+
     prev = pwkv[...]
-    keys = jnp.concatenate([prev[:, :64], own_k], axis=0)
-    values = jnp.concatenate([prev[:, 64:], own_v], axis=0)
+    keys = jnp.concatenate([prev[:, :64], own_pair[:, :64]], axis=0)
+    values = jnp.concatenate([prev[:, 64:], own_pair[:, 64:]], axis=0)
     q_row, k_col = iota((T, 2 * T), 0), iota((T, 2 * T), 1)
-    usable = (k_col > q_row) & (k_col <= q_row + T) & ((k_col >= T) | (sp > 0))
+    usable = (k_col > q_row) & (k_col <= q_row + T) & ((k_col >= T) | has_prev)
     outs = []
     for h in range(2):
         logit = dot_nt(query_w[:, 64 * h : 64 * h + 64], keys) * (0.125 * LOG2E)
         logit = jnp.where(usable, logit, -jnp.inf)
-        sink = sinks[h] * LOG2E
+        sink = sinks_s[h] * LOG2E
         top = jnp.maximum(jnp.max(logit, axis=1, keepdims=True), sink)
         weight = jnp.exp2(logit - top)
         norm = jnp.sum(weight, axis=1, keepdims=True) + jnp.exp2(sink - top)
@@ -202,14 +239,8 @@
             send = rcopy(ref, ref, s_k.at[4 + 2 * side + n], rsem, row_of(d))
             send.start()
             kv_sends.append(send)
-    for d in (1, 7, 3, 5):
-        src = (y + d) % NY
-        rcopy(kvb.at[src], kvb.at[src], s_k.at[0], r_k.at[src], row_of(1)).wait_recv()
-    far = (y + 4) % NY
-    for n in range(2):
-        rcopy(kvb.at[far, n], kvb.at[far, n], s_k.at[0], r_k4.at[n], row_of(1)).wait_recv()
-
-    def spread(j, _):
+
+    def spread(j):
         key_t, val = kvb[j, 0], kvb[j, 1]
         zero = jnp.zeros_like(key_t)
         feat = iota((T, 128), 0) < 64
@@ -218,41 +249,83 @@
         lane = iota((T, 128), 1) < 64
         vbd[j, :T, :] = jnp.where(lane, val, zero)
         vbd[j, T:, :] = jnp.where(lane, zero, val)
-        return 0
-
-    lax.fori_loop(0, NY, spread, 0)
-
-    bias_row = jnp.where(iota((1, 2 * T), 1) < T, bias[0] * LOG2E, bias[1] * LOG2E)
-
-    def tile(q, j, usable):
-        score = dot(q, kbd[j]) + bias_row
-        soft = jnp.maximum(score, jnp.log(1.0 + jnp.exp2(jnp.minimum(score, 126.0))) * LOG2E)
-        if usable is not None:
-            soft = jnp.where(usable, soft, 0.0)
-        soft_b = soft.astype(BF16)
-        weight = jnp.exp2((score - soft) - dot(soft_b, tri[...]))
-        if usable is not None:
-            weight = jnp.where(usable, weight, 0.0)
-        return dot(weight.astype(BF16), vbd[j]), dot(soft_b, ones[...])
-
-    def log_rows(total):
+
+    bias_row = jnp.where(iota((1, 2 * T), 1) < T, bias_s[0] * LOG2E, bias_s[1] * LOG2E)
+
+    def scores(q, pair, usable_of=None):
+        query = qb[q]
+        for t, j in enumerate(pair):
+            score = dot(query, kbd[j]) + bias_row
+            soft = jnp.maximum(score, jnp.log(1.0 + jnp.exp2(jnp.minimum(score, 126.0))) * LOG2E)
+            rest = score - soft
+            if usable_of is not None:
+                usable = usable_of(j)
+                soft = jnp.where(usable, soft, 0.0)
+                rest = jnp.where(usable, rest, -1e30)
+            diff[t] = rest
+            soft_b[t] = soft.astype(BF16)
+            sum0 = jnp.sum(soft[:, :T], axis=1, keepdims=True)
+            sum1 = jnp.sum(soft[:, T:], axis=1, keepdims=True)
+            logs[q, j] = jnp.where(iota((T, 128), 1) < 64, sum0, sum1)
+
+    def weights():
+        for t in range(2):
+            weight_b[t] = jnp.exp2(diff[t] - dot(soft_b[t], tri[...])).astype(BF16)
+
+    def outputs(q, pair):
+        for t, j in enumerate(pair):
+            parts[q, j] = dot(weight_b[t], vbd[j])
+
+    def visit(pair, first):
+        for j in pair:
+            spread(j)
+        scores(z, pair, lambda j: (j * T + k_col % T) < (y * T + q_row))
+
+        def step(q, _):
+            if first:
+                rcopy(qb.at[q], qb.at[q], s_q.at[0], r_q.at[q], (q * NY + y, tp)).wait_recv()
+            outputs(jnp.where(q - 2 < z, NZ, q - 2), pair)
+            weights()
+            scores(q, pair)
+            return 0
+
+        lax.fori_loop(z + 1, NZ, step, 0)
+        outputs(jnp.where(z == NZ - 1, NZ, NZ - 2), pair)
+        weights()
+        outputs(NZ - 1, pair)
+
+    weight_b[...] = jnp.zeros_like(weight_b)
+
+    def kv_wait(src):
+        rcopy(kvb.at[src], kvb.at[src], s_k.at[0], r_k.at[src], row_of(1)).wait_recv()
+
+    far = [(y + d) % NY for d in range(NY)]
+    visit((y, before), True)
+    kv_wait(far[NY - 1])
+    visit((after, far[NY - 1]), False)
+    kv_wait(far[1])
+    kv_wait(far[NY - 3])
+    visit((far[1], far[NY - 3]), False)
+    kv_wait(far[3])
+    for n in range(2):
+        rcopy(kvb.at[far[4], n], kvb.at[far[4], n], s_k.at[0], r_k4.at[n], row_of(1)).wait_recv()
+    visit((far[3], far[4]), False)
+
+    def total_of(q):
+        part, total = parts[q, NY - 1], logs[q, NY - 1]
+        for j in range(NY - 2, -1, -1):
+            part = part + jnp.exp2(-total) * parts[q, j]
+            total = total + logs[q, j]
         flipped = total.T
-        return flipped[0:1, :], flipped[64:65, :]
+        return part, (flipped[0:1, :], flipped[64:65, :])
 
     def p_send(to):
         return rcopy(pout.at[to], prec.at[z], s_p.at[to], r_p.at[z], (to * NY + y, tp))
 
-    def query_step(i, _):
+    def give(i, _):
         zq = NZ - 1 - i
-        rcopy(qb.at[zq], qb.at[zq], s_q.at[0], r_q.at[zq], (zq * NY + y, tp)).wait_recv()
-        q = qb[zq]
-        part, logs = tile(q, NY - 1, None)
-        for j in range(NY - 2, -1, -1):
-            p_j, l_j = tile(q, j, None)
-            part = part + jnp.exp2(-logs) * p_j
-            logs = logs + l_j
+        part, (l0, l1) = total_of(zq)
         pout[zq, :T, :] = part.astype(BF16)
-        l0, l1 = log_rows(logs)
         h0, h1 = l0.astype(BF16).astype(F32), l1.astype(BF16).astype(F32)
         row = iota((16, 128), 0)
         packed = jnp.where(row == 0, h0, jnp.where(row == 1, l0 - h0, jnp.where(row == 2, h1, l1 - h1)))
@@ -260,24 +333,12 @@
         p_send(zq).start()
         return 0
 
-    lax.fori_loop(0, NZ - 1 - z, query_step, 0)
-
-    acc_p[...] = jnp.zeros_like(acc_p)
-    acc_l[...] = jnp.zeros_like(acc_l)
-    own_q = qb[z]
-
-    def own_step(i, _):
-        j = NY - 1 - i
-        usable = (j * T + k_col % T) < (y * T + q_row)
-        p_j, l_j = tile(own_q, j, usable)
-        acc_p[...] += jnp.exp2(-acc_l[...]) * p_j
-        acc_l[...] += l_j
-        return 0
-
-    lax.fori_loop(NY - 1 - y, NY, own_step, 0)
-
-    def merge(i, logs):
-        l0, l1 = logs
+    lax.fori_loop(0, NZ - 1 - z, give, 0)
+    own_part, own_logs = total_of(z)
+    acc_p[...] = own_part
+
+    def merge(i, rows):
+        l0, l1 = rows
         src = z - 1 - i
         rcopy(pout.at[src], prec.at[src], s_p.at[0], r_p.at[src], (src * NY + y, tp)).wait_recv()
         factor = jnp.concatenate(
@@ -287,7 +348,7 @@
         more = prec[src, T:, :].astype(F32)
         return l0 + (more[0:1] + more[1:2]), l1 + (more[2:3] + more[3:4])
 
-    lax.fori_loop(0, z, merge, log_rows(acc_l[...]))
+    lax.fori_loop(0, z, merge, own_logs)
 
     stick_out = acc_p[...].astype(BF16).astype(F32)
     with_squares(ab, stick_out)
@@ -311,8 +372,13 @@
     mean = jnp.sum(combined * combined, axis=1, keepdims=True) * (1.0 / D)
     out[...] = (combined * lax.rsqrt(mean + EPS) * post_v[...]).astype(BF16)
 
-    for send in tok_sends + kv_sends + [win_send] + win_sends + stick_sends:
+    for send in tok_sends + kv_sends + win_sends + stick_sends:
         send.wait_send()
+
+    @pl.when(has_next)
+    def _():
+        win_send.wait_send()
+
     for n in (4, 5, 6):
         rcopy(own_tok, own_tok, s_a.at[n], r_a.at[tp], (sp, partner)).wait_send()
 
@@ -334,33 +400,33 @@
     stick_bias, sinks, stick_gain, window_gain, w_out_stick, w_out_window, post_gain,
 ):
     anywhere = pl.BlockSpec(memory_space=pl.ANY)
-    scalars = pl.BlockSpec(memory_space=pltpu.SMEM)
     dma = pltpu.SemaphoreType.DMA
     vm = pltpu.VMEM
     scratch = [
-        vm((NTP, T, CH), BF16), vm((D, 512), BF16), vm((D, 64), BF16), vm((D, 64), BF16),
+        vm((NTP, T, CH), BF16), vm((D, 512), BF16), vm((128, D), BF16),
         vm((128, D), BF16), vm((128, D), BF16), vm((1, D), F32), vm((1, 128), F32), vm((1, 128), F32), vm((1, D), F32),
-        vm((T, 512), F32), vm((T, 64), F32), vm((T, 64), F32), vm((T, 128), F32),
+        vm((T, 512), F32), vm((T, 128), F32), vm((T, 128), F32),
         vm((NY, 2, T, 128), BF16), vm((NZ, T, 128), BF16), vm((NY, 128, 2 * T), BF16), vm((NY, 2 * T, 128), BF16),
-        vm((256, 256), BF16), vm((256, 128), BF16),
+        vm((256, 256), BF16), vm((2, T, 2 * T), BF16), vm((2, T, 2 * T), F32), vm((2, T, 2 * T), BF16),
+        vm((NZ + 1, NY, T, 128), F32), vm((NZ + 1, NY, T, 128), F32),
         vm((T, 128), BF16), vm((T, 128), BF16), vm((NZ, PROWS, 128), BF16), vm((NZ, PROWS, 128), BF16),
-        vm((T, 128), F32), vm((T, 128), F32), vm((T, PACK), BF16), vm((T, PACK), BF16),
-        vm((NTP, 16, PACK), BF16), vm((NTP, 16, PACK), BF16),
-        dma((13,)), dma((7,)), dma((NTP,)), dma((8,)), dma((NY,)), dma((2,)), dma((NZ,)), dma((NZ,)), dma, dma,
+        vm((T, 128), F32), vm((T, PACK), BF16), vm((T, PACK), BF16),
+        vm((NTP, 16, PACK), BF16), vm((NTP, 16, PACK), BF16), pltpu.SMEM((2,), F32), pltpu.SMEM((2,), F32),
+        dma((15,)), dma((7,)), dma((NTP,)), dma((8,)), dma((NY,)), dma((2,)), dma((NZ,)), dma((NZ,)), dma, dma, pltpu.SemaphoreType.REGULAR,
         dma((NZ,)), dma((NZ,)), dma((NTP,)), dma((NTP,)), dma((NTP,)), dma((NTP,)),
     ]
     return pl.pallas_call(
         kernel,
         out_shape=jax.ShapeDtypeStruct((T // NTP, D), BF16),
-        in_specs=[anywhere] * 8 + [scalars] * 2 + [anywhere] * 5,
+        in_specs=[anywhere] * 15,
         out_specs=pl.BlockSpec(memory_space=pltpu.VMEM),
         scratch_shapes=scratch,
         compiler_params=pltpu.CompilerParams(
-            collective_id=0, has_side_effects=True, vmem_limit_bytes=48 * 1024 * 1024
+            collective_id=0, has_side_effects=True, vmem_limit_bytes=60 * 1024 * 1024
         ),
     )(
         tokens, pre_gain.reshape(1, -1), w_query_stick, w_key_stick, w_value_stick, w_query_window,
-        w_key_window, w_value_window, stick_bias, sinks, stick_gain.reshape(1, -1), window_gain.reshape(1, -1),
+        w_key_window.T, w_value_window.T, stick_bias, sinks, stick_gain.reshape(1, -1), window_gain.reshape(1, -1),
         w_out_stick, w_out_window, post_gain.reshape(1, -1),
     )
 

time: 75.8 us -> 54.5 us (0.72)
  the two profiles are of different devices: /device:TPU:48 before, /device:TPU:193 now
where the time goes in v2:
time: 54.5 us; the launch traced here: 54.3 us
  Pallas kernels  52.8 us (97%)
  local copies, waits for them, and re-layouts  1.47 us (3%)
    pallas_call x1, Pallas kernels, shards(): pl.pallas_call(kernel, out_shape=jax.ShapeDtypeStruct((T // NTP, D), BF16...  52.8 us
    unnamed x1, local copies, waits for them, and re-layouts  1.47 us

profile of v2, /device:TPU:193, one launch (start us, length us, event | category | flops | bytes accessed | tf_op | source)
XLA Modules:
  0.0 54.3 jit_solution(3169812635997073130)
XLA Ops:
  0.0 52.8 %shard_map.145 = bf16[16,2048]{1,0:T(8,128)(2,1)} custom-call(bf16[128,256]{1,0:T(8,128)(2,1)} %tok.1, f32[1,2048]{1,0:T(1,128)} %bitcast.8, bf16[2048,128]{1,0:T(8,128)(2,1)} %wqs.1, bf16[2048,128]{1,0:T(8,128)(2,1)} %wks.1, bf16[2048,128]{1,0:T(8,128)(2,1)} %wvs.1, bf16[2048,128]{1,0:T(8,128)(2,1)} %wqw.1, bf16[64,2048]{1,0:T(8,128)(2,1)} %bitcast.6, ...), custom_call_target="tpu_custom_call" | custom-call | tf_op jit(solution)/shard_map/pallas_call | solution.py:418
  52.8 1.5 %copy.17 = bf16[16,2048]{1,0:T(8,128)(2,1)} copy(bf16[16,2048]{1,0:T(8,128)(2,1)} %shard_map.145) | data formatting | bytes 131072

commit v3 on v2

--- a/solution.py
+++ b/solution.py
@@ -46,7 +46,7 @@
     tok, pre, wqs, wks, wvs, wqw, wkw, wvw, bias, sinks, sgain, wgain, wos, wow, post,
     out,
     tok_all, w4, w_win, wo_s, wo_w, pre_v, sg_v, wg_v, post_v,
-    acc4, acc_w, sq, kvb, qb, kbd, vbd, tri, soft_b, diff, weight_b, parts, logs,
+    acc4, acc_w, sq, kvb, qb, kbd, vbd, tri, raw, soft_b, diff, expo, weight_b, parts, logs,
     wkv, pwkv, pout, prec, acc_p, ab, bb, ra, rb, bias_s, sinks_s,
     lsem, s_a, r_a, s_k, r_k, r_k4, s_q, r_q, s_w, r_w, ready, s_p, r_p, s_ra, r_ra, s_rb, r_rb,
 ):
@@ -61,6 +61,9 @@
         return pltpu.make_async_remote_copy(
             src_ref=src, dst_ref=dst, send_sem=ssem, recv_sem=rsem, device_id=dev, device_id_type=MESH
         )
+
+    def rows_of(block, count=1):
+        return pl.ds(pl.multiple_of(block * T, T), count * T)
 
     loads = [pltpu.make_async_copy(tok, tok_all.at[tp], lsem.at[0])]
     pairs = [
@@ -105,6 +108,9 @@
     acc4[...] = jnp.zeros_like(acc4)
     acc_w[...] = jnp.zeros_like(acc_w)
     sq[...] = jnp.zeros_like(sq)
+    for ref in (raw, soft_b, diff, expo, weight_b):
+        ref[...] = jnp.zeros_like(ref)
+    qb[NZ * T :, :] = jnp.zeros((T, 128), BF16)
 
     pl.semaphore_wait(barrier, len(greeted) + z + jnp.where(starts_row, 1, 0))
 
@@ -172,10 +178,10 @@
         kv_sends.append(rcopy(own_kv, own_kv, s_k.at[n], r_k.at[y], (z * NY + (y + d) % NY, tp)))
     for send in kv_sends:
         send.start()
-    qb[z] = (acc4[:, 256:384] * (inv * (0.125 * LOG2E))).astype(BF16)
+    qb[rows_of(z), :] = (acc4[:, 256:384] * (inv * (0.125 * LOG2E))).astype(BF16)
 
     def q_send(i):
-        return rcopy(qb.at[z], qb.at[z], s_q.at[i], r_q.at[z], (i * NY + y, tp))
+        return rcopy(qb.at[rows_of(z), :], qb.at[rows_of(z), :], s_q.at[i], r_q.at[z], (i * NY + y, tp))
 
     def q_start(i, _):
         q_send(i).start()
@@ -252,70 +258,102 @@
 
     bias_row = jnp.where(iota((1, 2 * T), 1) < T, bias_s[0] * LOG2E, bias_s[1] * LOG2E)
 
-    def scores(q, pair, usable_of=None):
-        query = qb[q]
-        for t, j in enumerate(pair):
-            score = dot(query, kbd[j]) + bias_row
+    in_head0 = iota((2 * T, 128), 1) < 64
+    far = [(y + d) % NY for d in range(NY)]
+    query_pairs = (NZ - z + 1) // 2
+    early = jnp.minimum(query_pairs, 2)
+    late = query_pairs - early
+    units = 4 * query_pairs
+
+    def unit(i):
+        at = jnp.clip(i, 0, units - 1)
+        rest = jnp.maximum(at - 3 * early, 0)
+        width = jnp.maximum(late, 1)
+        in_early, in_last = at < 3 * early, at >= 3 * query_pairs
+        k = jnp.where(in_early, at // early, jnp.where(in_last, 3, rest // width))
+        p = jnp.where(in_early, at % early, jnp.where(in_last, at - 3 * query_pairs, early + rest % width))
+        first = jnp.where(k == 0, y, jnp.where(k == 1, after, jnp.where(k == 2, far[1], far[3])))
+        second = jnp.where(k == 0, before, jnp.where(k == 1, far[7], jnp.where(k == 2, far[5], far[4])))
+        rows = rows_of(jnp.where((i >= 0) & (i < units), z + 2 * p, NZ + 1), 2)
+        return p, (first, second), rows
+
+    halves = (pl.ds(0, 2 * T), pl.ds(2 * T, 2 * T))
+
+    def kv_wait(src):
+        rcopy(kvb.at[src], kvb.at[src], s_k.at[0], r_k.at[src], row_of(1)).wait_recv()
+
+    def await_queries(p):
+        for n in range(2):
+            q = z + 2 * p + n
+
+            @pl.when((q > z) & (q < NZ))
+            def _(q=q):
+                block = qb.at[rows_of(q), :]
+                rcopy(block, block, s_q.at[0], r_q.at[q], (q * NY + y, tp)).wait_recv()
+
+    def unit_step(i, _):
+        p, pair, rows = unit(i)
+
+        @pl.when((i < early) | ((i >= 3 * early) & (i < 3 * early + late)))
+        def _():
+            await_queries(p)
+
+        @pl.when(i == early)
+        def _():
+            kv_wait(far[7])
+            spread(far[7])
+
+        @pl.when(i == 2 * early)
+        def _():
+            for d in (1, 5):
+                kv_wait(far[d])
+                spread(far[d])
+
+        @pl.when(i == 3 * query_pairs)
+        def _():
+            kv_wait(far[3])
+            spread(far[3])
+            for n in range(2):
+                rcopy(kvb.at[far[4], n], kvb.at[far[4], n], s_k.at[0], r_k4.at[n], row_of(1)).wait_recv()
+            spread(far[4])
+
+        _, pair_d, rows_d = unit(i - 4)
+        for half, j in zip(halves, pair_d):
+            parts[j, rows_d, :] = dot(weight_b[half, :], vbd[j])
+        weight_b[...] = jnp.exp2(expo[...]).astype(BF16)
+        expo[...] = diff[...] - dot(soft_b[...], tri[...])
+        _, pair_b, rows_b = unit(i - 1)
+        for half, j in zip(halves, pair_b):
+            score = raw[half, :] + bias_row
             soft = jnp.maximum(score, jnp.log(1.0 + jnp.exp2(jnp.minimum(score, 126.0))) * LOG2E)
-            rest = score - soft
-            if usable_of is not None:
-                usable = usable_of(j)
-                soft = jnp.where(usable, soft, 0.0)
-                rest = jnp.where(usable, rest, -1e30)
-            diff[t] = rest
-            soft_b[t] = soft.astype(BF16)
+            diff[half, :] = score - soft
+            soft_b[half, :] = soft.astype(BF16)
             sum0 = jnp.sum(soft[:, :T], axis=1, keepdims=True)
             sum1 = jnp.sum(soft[:, T:], axis=1, keepdims=True)
-            logs[q, j] = jnp.where(iota((T, 128), 1) < 64, sum0, sum1)
-
-    def weights():
-        for t in range(2):
-            weight_b[t] = jnp.exp2(diff[t] - dot(soft_b[t], tri[...])).astype(BF16)
-
-    def outputs(q, pair):
-        for t, j in enumerate(pair):
-            parts[q, j] = dot(weight_b[t], vbd[j])
-
-    def visit(pair, first):
-        for j in pair:
-            spread(j)
-        scores(z, pair, lambda j: (j * T + k_col % T) < (y * T + q_row))
-
-        def step(q, _):
-            if first:
-                rcopy(qb.at[q], qb.at[q], s_q.at[0], r_q.at[q], (q * NY + y, tp)).wait_recv()
-            outputs(jnp.where(q - 2 < z, NZ, q - 2), pair)
-            weights()
-            scores(q, pair)
-            return 0
-
-        lax.fori_loop(z + 1, NZ, step, 0)
-        outputs(jnp.where(z == NZ - 1, NZ, NZ - 2), pair)
-        weights()
-        outputs(NZ - 1, pair)
-
-    weight_b[...] = jnp.zeros_like(weight_b)
-
-    def kv_wait(src):
-        rcopy(kvb.at[src], kvb.at[src], s_k.at[0], r_k.at[src], row_of(1)).wait_recv()
-
-    far = [(y + d) % NY for d in range(NY)]
-    visit((y, before), True)
-    kv_wait(far[NY - 1])
-    visit((after, far[NY - 1]), False)
-    kv_wait(far[1])
-    kv_wait(far[NY - 3])
-    visit((far[1], far[NY - 3]), False)
-    kv_wait(far[3])
-    for n in range(2):
-        rcopy(kvb.at[far[4], n], kvb.at[far[4], n], s_k.at[0], r_k4.at[n], row_of(1)).wait_recv()
-    visit((far[3], far[4]), False)
+            logs[j, rows_b, :] = jnp.where(in_head0, sum0, sum1)
+        own_rows = rows_of(jnp.minimum(z + 2 * p, NZ - 1), 2)
+        for half, j in zip(halves, pair):
+            raw[half, :] = dot(qb[own_rows, :], kbd[j])
+
+        @pl.when(p == 0)
+        def _():
+            for n, j in enumerate(pair):
+                mine = pl.ds(2 * T * n, T)
+                raw[mine, :] = jnp.where(k_col % T - q_row < (y - j) * T, raw[mine, :], -1e30)
+
+        return 0
+
+    spread(y)
+    spread(before)
+    spread(after)
+    lax.fori_loop(0, units + 4, unit_step, 0)
 
     def total_of(q):
-        part, total = parts[q, NY - 1], logs[q, NY - 1]
+        rows = rows_of(q)
+        part, total = parts[NY - 1, rows, :], logs[NY - 1, rows, :]
         for j in range(NY - 2, -1, -1):
-            part = part + jnp.exp2(-total) * parts[q, j]
-            total = total + logs[q, j]
+            part = part + jnp.exp2(-total) * parts[j, rows, :]
+            total = total + logs[j, rows, :]
         flipped = total.T
         return part, (flipped[0:1, :], flipped[64:65, :])
 
@@ -406,9 +444,10 @@
         vm((NTP, T, CH), BF16), vm((D, 512), BF16), vm((128, D), BF16),
         vm((128, D), BF16), vm((128, D), BF16), vm((1, D), F32), vm((1, 128), F32), vm((1, 128), F32), vm((1, D), F32),
         vm((T, 512), F32), vm((T, 128), F32), vm((T, 128), F32),
-        vm((NY, 2, T, 128), BF16), vm((NZ, T, 128), BF16), vm((NY, 128, 2 * T), BF16), vm((NY, 2 * T, 128), BF16),
-        vm((256, 256), BF16), vm((2, T, 2 * T), BF16), vm((2, T, 2 * T), F32), vm((2, T, 2 * T), BF16),
-        vm((NZ + 1, NY, T, 128), F32), vm((NZ + 1, NY, T, 128), F32),
+        vm((NY, 2, T, 128), BF16), vm(((NZ + 1) * T, 128), BF16), vm((NY, 128, 2 * T), BF16), vm((NY, 2 * T, 128), BF16),
+        vm((256, 256), BF16), vm((4 * T, 2 * T), F32), vm((4 * T, 2 * T), BF16), vm((4 * T, 2 * T), F32), vm((4 * T, 2 * T), F32),
+        vm((4 * T, 2 * T), BF16),
+        vm((NY, (NZ + 3) * T, 128), F32), vm((NY, (NZ + 3) * T, 128), F32),
         vm((T, 128), BF16), vm((T, 128), BF16), vm((NZ, PROWS, 128), BF16), vm((NZ, PROWS, 128), BF16),
         vm((T, 128), F32), vm((T, PACK), BF16), vm((T, PACK), BF16),
         vm((NTP, 16, PACK), BF16), vm((NTP, 16, PACK), BF16), pltpu.SMEM((2,), F32), pltpu.SMEM((2,), F32),

time: 54.5 us -> 50.1 us (0.919)
  the two profiles are of different devices: /device:TPU:193 before, /device:TPU:144 now
where the time goes in v3:
time: 50.1 us; the launch traced here: 49.9 us
  Pallas kernels  48.4 us (97%)
  local copies, waits for them, and re-layouts  1.47 us (3%)
    pallas_call x1, Pallas kernels, shards(): pl.pallas_call(kernel, out_shape=jax.ShapeDtypeStruct((T // NTP, D), BF16...  48.4 us
    unnamed x1, local copies, waits for them, and re-layouts  1.47 us

profile of v3, /device:TPU:144, one launch (start us, length us, event | category | flops | bytes accessed | tf_op | source)
XLA Modules:
  0.0 49.9 jit_solution(17392935914925618482)
XLA Ops:
  0.0 48.4 %shard_map.145 = bf16[16,2048]{1,0:T(8,128)(2,1)} custom-call(bf16[128,256]{1,0:T(8,128)(2,1)} %tok.1, f32[1,2048]{1,0:T(1,128)} %bitcast.8, bf16[2048,128]{1,0:T(8,128)(2,1)} %wqs.1, bf16[2048,128]{1,0:T(8,128)(2,1)} %wks.1, bf16[2048,128]{1,0:T(8,128)(2,1)} %wvs.1, bf16[2048,128]{1,0:T(8,128)(2,1)} %wqw.1, bf16[64,2048]{1,0:T(8,128)(2,1)} %bitcast.6, ...), custom_call_target="tpu_custom_call" | custom-call | tf_op jit(solution)/shard_map/pallas_call | solution.py:457
  48.4 1.5 %copy.17 = bf16[16,2048]{1,0:T(8,128)(2,1)} copy(bf16[16,2048]{1,0:T(8,128)(2,1)} %shard_map.145) | data formatting | bytes 131072

commit v4 on v3

--- a/solution.py
+++ b/solution.py
@@ -46,7 +46,7 @@
     tok, pre, wqs, wks, wvs, wqw, wkw, wvw, bias, sinks, sgain, wgain, wos, wow, post,
     out,
     tok_all, w4, w_win, wo_s, wo_w, pre_v, sg_v, wg_v, post_v,
-    acc4, acc_w, sq, kvb, qb, kbd, vbd, tri, raw, soft_b, diff, expo, weight_b, parts, logs,
+    acc4, acc_w, sq, kvb, qb, kbd, vbd, tri, raw, soft_b, diff, expo, weight_b, parts, logs, offset,
     wkv, pwkv, pout, prec, acc_p, ab, bb, ra, rb, bias_s, sinks_s,
     lsem, s_a, r_a, s_k, r_k, r_k4, s_q, r_q, s_w, r_w, ready, s_p, r_p, s_ra, r_ra, s_rb, r_rb,
 ):
@@ -105,6 +105,7 @@
 
     row2, col2 = iota((256, 256), 0), iota((256, 256), 1)
     tri[...] = jnp.where((row2 > col2) & (row2 // T == col2 // T), 1.0, 0.0).astype(BF16)
+    offset[...] = iota((T, 2 * T), 1) % T - iota((T, 2 * T), 0)
     acc4[...] = jnp.zeros_like(acc4)
     acc_w[...] = jnp.zeros_like(acc_w)
     sq[...] = jnp.zeros_like(sq)
@@ -262,20 +263,18 @@
     far = [(y + d) % NY for d in range(NY)]
     query_pairs = (NZ - z + 1) // 2
     early = jnp.minimum(query_pairs, 2)
-    late = query_pairs - early
     units = 4 * query_pairs
 
     def unit(i):
         at = jnp.clip(i, 0, units - 1)
-        rest = jnp.maximum(at - 3 * early, 0)
-        width = jnp.maximum(late, 1)
-        in_early, in_last = at < 3 * early, at >= 3 * query_pairs
-        k = jnp.where(in_early, at // early, jnp.where(in_last, 3, rest // width))
-        p = jnp.where(in_early, at % early, jnp.where(in_last, at - 3 * query_pairs, early + rest % width))
+        mid, rest = at - 2 * early, jnp.maximum(at - 4 * early, 0)
+        p = jnp.where(mid < 0, at // 2, jnp.where(mid < 2 * early, early - 1 - mid // 2, early + rest // 4))
+        k = jnp.where(mid < 0, at % 2, jnp.where(mid < 2 * early, 2 + mid % 2, rest % 4))
+        real = (i >= 0) & (i < units)
         first = jnp.where(k == 0, y, jnp.where(k == 1, after, jnp.where(k == 2, far[1], far[3])))
         second = jnp.where(k == 0, before, jnp.where(k == 1, far[7], jnp.where(k == 2, far[5], far[4])))
-        rows = rows_of(jnp.where((i >= 0) & (i < units), z + 2 * p, NZ + 1), 2)
-        return p, (first, second), rows
+        rows = rows_of(jnp.where(real, z + 2 * p, NZ + 1), 2)
+        return p, k, real, (first, second), rows
 
     halves = (pl.ds(0, 2 * T), pl.ds(2 * T, 2 * T))
 
@@ -290,63 +289,6 @@
             def _(q=q):
                 block = qb.at[rows_of(q), :]
                 rcopy(block, block, s_q.at[0], r_q.at[q], (q * NY + y, tp)).wait_recv()
-
-    def unit_step(i, _):
-        p, pair, rows = unit(i)
-
-        @pl.when((i < early) | ((i >= 3 * early) & (i < 3 * early + late)))
-        def _():
-            await_queries(p)
-
-        @pl.when(i == early)
-        def _():
-            kv_wait(far[7])
-            spread(far[7])
-
-        @pl.when(i == 2 * early)
-        def _():
-            for d in (1, 5):
-                kv_wait(far[d])
-                spread(far[d])
-
-        @pl.when(i == 3 * query_pairs)
-        def _():
-            kv_wait(far[3])
-            spread(far[3])
-            for n in range(2):
-                rcopy(kvb.at[far[4], n], kvb.at[far[4], n], s_k.at[0], r_k4.at[n], row_of(1)).wait_recv()
-            spread(far[4])
-
-        _, pair_d, rows_d = unit(i - 4)
-        for half, j in zip(halves, pair_d):
-            parts[j, rows_d, :] = dot(weight_b[half, :], vbd[j])
-        weight_b[...] = jnp.exp2(expo[...]).astype(BF16)
-        expo[...] = diff[...] - dot(soft_b[...], tri[...])
-        _, pair_b, rows_b = unit(i - 1)
-        for half, j in zip(halves, pair_b):
-            score = raw[half, :] + bias_row
-            soft = jnp.maximum(score, jnp.log(1.0 + jnp.exp2(jnp.minimum(score, 126.0))) * LOG2E)
-            diff[half, :] = score - soft
-            soft_b[half, :] = soft.astype(BF16)
-            sum0 = jnp.sum(soft[:, :T], axis=1, keepdims=True)
-            sum1 = jnp.sum(soft[:, T:], axis=1, keepdims=True)
-            logs[j, rows_b, :] = jnp.where(in_head0, sum0, sum1)
-        own_rows = rows_of(jnp.minimum(z + 2 * p, NZ - 1), 2)
-        for half, j in zip(halves, pair):
-            raw[half, :] = dot(qb[own_rows, :], kbd[j])
-
-        @pl.when(p == 0)
-        def _():
-            for n, j in enumerate(pair):
-                mine = pl.ds(2 * T * n, T)
-                raw[mine, :] = jnp.where(k_col % T - q_row < (y - j) * T, raw[mine, :], -1e30)
-
-        return 0
-
-    spread(y)
-    spread(before)
-    spread(after)
-    lax.fori_loop(0, units + 4, unit_step, 0)
 
     def total_of(q):
         rows = rows_of(q)
@@ -360,8 +302,7 @@
     def p_send(to):
         return rcopy(pout.at[to], prec.at[z], s_p.at[to], r_p.at[z], (to * NY + y, tp))
 
-    def give(i, _):
-        zq = NZ - 1 - i
+    def give(zq):
         part, (l0, l1) = total_of(zq)
         pout[zq, :T, :] = part.astype(BF16)
         h0, h1 = l0.astype(BF16).astype(F32), l1.astype(BF16).astype(F32)
@@ -369,9 +310,72 @@
         packed = jnp.where(row == 0, h0, jnp.where(row == 1, l0 - h0, jnp.where(row == 2, h1, l1 - h1)))
         pout[zq, T:, :] = packed.astype(BF16)
         p_send(zq).start()
-        return 0
-
-    lax.fori_loop(0, NZ - 1 - z, give, 0)
+
+    def unit_step(i, now):
+        later = 1 - now
+        _, _, _, pair_d, rows_d = unit(i - 4)
+        p, _, _, pair, _ = unit(i)
+        for half, j in zip(halves, pair_d):
+            parts[j, rows_d, :] = dot(weight_b[now, half, :], vbd[j])
+        weight_b[later] = jnp.exp2(expo[now]).astype(BF16)
+        expo[later] = diff[now] - dot(soft_b[now], tri[...])
+        _, _, _, pair_b, rows_b = unit(i - 1)
+        for half, j in zip(halves, pair_b):
+            score = raw[now, half, :] + bias_row
+            soft = jnp.maximum(score, jnp.log(1.0 + jnp.exp2(jnp.minimum(score, 126.0))) * LOG2E)
+            diff[later, half, :] = score - soft
+            soft_b[later, half, :] = soft.astype(BF16)
+            sum0 = jnp.sum(soft[:, :T], axis=1, keepdims=True)
+            sum1 = jnp.sum(soft[:, T:], axis=1, keepdims=True)
+            logs[j, rows_b, :] = jnp.where(in_head0, sum0, sum1)
+        own_rows = rows_of(jnp.minimum(z + 2 * p, NZ - 1), 2)
+        for half, j in zip(halves, pair):
+            score = dot(qb[own_rows, :], kbd[j])
+            limit = jnp.where(p == 0, (y - j) * T, NY * T)
+            raw[later, pl.ds(half.start, T), :] = jnp.where(offset[...] < limit, score[:T], -1e30)
+            raw[later, pl.ds(half.start + T, T), :] = score[T:]
+
+    def give_done(i):
+        p_d, k_d, real_d, _, _ = unit(i)
+        for n in range(2):
+            q_d = z + 2 * p_d + n
+
+            @pl.when(real_d & (k_d == 3) & (q_d > z) & (q_d < NZ))
+            def _(q_d=q_d):
+                give(q_d)
+
+    def two_steps(i, _):
+        first = 2 * i
+        p, k, _, _, _ = unit(first)
+
+        @pl.when((k == 0) & (first < units))
+        def _():
+            await_queries(p)
+
+        @pl.when(i == 0)
+        def _():
+            kv_wait(far[7])
+            spread(far[7])
+
+        @pl.when(i == early)
+        def _():
+            for d in (1, 5, 3):
+                kv_wait(far[d])
+                spread(far[d])
+            for n in range(2):
+                rcopy(kvb.at[far[4], n], kvb.at[far[4], n], s_k.at[0], r_k4.at[n], row_of(1)).wait_recv()
+            spread(far[4])
+
+        unit_step(first, 0)
+        unit_step(first + 1, 1)
+        give_done(first - 3)
+        return 0
+
+    spread(y)
+    spread(before)
+    spread(after)
+    lax.fori_loop(0, 2 * query_pairs + 2, two_steps, 0)
+
     own_part, own_logs = total_of(z)
     acc_p[...] = own_part
 
@@ -445,9 +449,9 @@
         vm((128, D), BF16), vm((128, D), BF16), vm((1, D), F32), vm((1, 128), F32), vm((1, 128), F32), vm((1, D), F32),
         vm((T, 512), F32), vm((T, 128), F32), vm((T, 128), F32),
         vm((NY, 2, T, 128), BF16), vm(((NZ + 1) * T, 128), BF16), vm((NY, 128, 2 * T), BF16), vm((NY, 2 * T, 128), BF16),
-        vm((256, 256), BF16), vm((4 * T, 2 * T), F32), vm((4 * T, 2 * T), BF16), vm((4 * T, 2 * T), F32), vm((4 * T, 2 * T), F32),
-        vm((4 * T, 2 * T), BF16),
-        vm((NY, (NZ + 3) * T, 128), F32), vm((NY, (NZ + 3) * T, 128), F32),
+        vm((256, 256), BF16), vm((2, 4 * T, 2 * T), F32), vm((2, 4 * T, 2 * T), BF16), vm((2, 4 * T, 2 * T), F32),
+        vm((2, 4 * T, 2 * T), F32), vm((2, 4 * T, 2 * T), BF16),
+        vm((NY, (NZ + 3) * T, 128), F32), vm((NY, (NZ + 3) * T, 128), F32), vm((T, 2 * T), jnp.int32),
         vm((T, 128), BF16), vm((T, 128), BF16), vm((NZ, PROWS, 128), BF16), vm((NZ, PROWS, 128), BF16),
         vm((T, 128), F32), vm((T, PACK), BF16), vm((T, PACK), BF16),
         vm((NTP, 16, PACK), BF16), vm((NTP, 16, PACK), BF16), pltpu.SMEM((2,), F32), pltpu.SMEM((2,), F32),

time: 50.1 us -> 45.4 us (0.906)
  the two profiles are of different devices: /device:TPU:144 before, /device:TPU:257 now
where the time goes in v4:
time: 45.4 us; the launch traced here: 44.9 us
  Pallas kernels  43.4 us (96%)
  local copies, waits for them, and re-layouts  1.47 us (3%)
    pallas_call x1, Pallas kernels, shards(): pl.pallas_call(kernel, out_shape=jax.ShapeDtypeStruct((T // NTP, D), BF16...  43.4 us
    unnamed x1, local copies, waits for them, and re-layouts  1.47 us

profile of v4, /device:TPU:257, one launch (start us, length us, event | category | flops | bytes accessed | tf_op | source)
XLA Modules:
  0.0 44.9 jit_solution(3966070942282229703)
XLA Ops:
  0.0 43.4 %shard_map.145 = bf16[16,2048]{1,0:T(8,128)(2,1)} custom-call(bf16[128,256]{1,0:T(8,128)(2,1)} %tok.1, f32[1,2048]{1,0:T(1,128)} %bitcast.8, bf16[2048,128]{1,0:T(8,128)(2,1)} %wqs.1, bf16[2048,128]{1,0:T(8,128)(2,1)} %wks.1, bf16[2048,128]{1,0:T(8,128)(2,1)} %wvs.1, bf16[2048,128]{1,0:T(8,128)(2,1)} %wqw.1, bf16[64,2048]{1,0:T(8,128)(2,1)} %bitcast.6, ...), custom_call_target="tpu_custom_call" | custom-call | tf_op jit(solution)/shard_map/pallas_call | solution.py:461
  43.4 1.5 %copy.17 = bf16[16,2048]{1,0:T(8,128)(2,1)} copy(bf16[16,2048]{1,0:T(8,128)(2,1)} %shard_map.145) | data formatting | bytes 131072

commit v5 on v4

--- a/solution.py
+++ b/solution.py
@@ -35,11 +35,10 @@
     return lax.broadcasted_iota(jnp.int32, shape, dim)
 
 
-def with_squares(ref, out):
-    total = jnp.sum(out * out, axis=1, keepdims=True)
+def split(total):
     high = total.astype(BF16).astype(F32)
-    lane = iota((T, 128), 1)
-    ref[:, D:] = jnp.where(lane == 0, high, jnp.where(lane == 1, total - high, 0.0)).astype(BF16)
+    lane = iota((total.shape[0], 128), 1)
+    return jnp.where(lane == 0, high, jnp.where(lane == 1, total - high, 0.0)).astype(BF16)
 
 
 def kernel(
@@ -47,8 +46,9 @@
     out,
     tok_all, w4, w_win, wo_s, wo_w, pre_v, sg_v, wg_v, post_v,
     acc4, acc_w, sq, kvb, qb, kbd, vbd, tri, raw, soft_b, diff, expo, weight_b, parts, logs, offset,
-    wkv, pwkv, pout, prec, acc_p, ab, bb, ra, rb, bias_s, sinks_s,
-    lsem, s_a, r_a, s_k, r_k, r_k4, s_q, r_q, s_w, r_w, ready, s_p, r_p, s_ra, r_ra, s_rb, r_rb,
+    wkv, pwkv, pout, prec, acc_p, ab, bb, ra, rb, mix_a, mix_b, in_a, in_b, bias_s, sinks_s,
+    lsem, s_a, r_a, s_k, r_k, r_k2, r_k3, r_k4, s_q, r_q, s_w, r_w, ready, s_p, r_p, s_ra, r_ra, s_rb, r_rb,
+    s_pair, r_pair,
 ):
     sp = lax.axis_index("sp")
     tp = lax.axis_index("tp")
@@ -70,7 +70,7 @@
         (pre, pre_v), (wks, w4.at[:, pl.ds(0, 128)]), (wvs, w4.at[:, pl.ds(128, 128)]),
         (wqs, w4.at[:, pl.ds(256, 128)]), (wqw, w4.at[:, pl.ds(384, 128)]),
         (wkw, w_win.at[pl.ds(0, 64), :]), (wvw, w_win.at[pl.ds(64, 64), :]),
-        (bias, bias_s), (sinks, sinks_s), (sgain, sg_v), (wgain, wg_v), (post, post_v), (wos, wo_s), (wow, wo_w),
+        (bias, bias_s), (sinks, sinks_s), (sgain, sg_v), (wgain, wg_v), (post, post_v), (wos, wo_s.at[c]), (wow, wo_w.at[c]),
     ]
     for n, (src, dst) in enumerate(pairs):
         loads.append(pltpu.make_async_copy(src, dst, lsem.at[n + 1]))
@@ -174,9 +174,14 @@
     kvb[y, 0] = (acc4[:, 0:128] * inv).T.astype(BF16)
     kvb[y, 1] = (acc4[:, 128:256] * inv).astype(BF16)
     own_kv = kvb.at[y]
+    row_of = lambda d: (z * NY + (y + d) % NY, tp)
     kv_sends = []
-    for n, d in enumerate((2, NY - 2, 1, NY - 1)):
-        kv_sends.append(rcopy(own_kv, own_kv, s_k.at[n], r_k.at[y], (z * NY + (y + d) % NY, tp)))
+    for plane in range(2):
+        for side, d in enumerate((2, NY - 2)):
+            ref = kvb.at[y, plane]
+            kv_sends.append(rcopy(ref, ref, s_k.at[2 * plane + side], r_k2.at[side, plane], row_of(d)))
+    for n, d in enumerate((1, NY - 1)):
+        kv_sends.append(rcopy(own_kv, own_kv, s_k.at[4 + n], r_k.at[y], row_of(d)))
     for send in kv_sends:
         send.start()
     qb[rows_of(z), :] = (acc4[:, 256:384] * (inv * (0.125 * LOG2E))).astype(BF16)
@@ -190,9 +195,15 @@
 
     lax.fori_loop(0, z, q_start, 0)
 
-    query_w = (acc4[:, 384:512] * inv).astype(BF16)
     for load in loads[8:]:
         load.wait()
+    pair_sends = []
+    for n, ref in enumerate((wo_w.at[c], wo_s.at[c])):
+        pair_sends.append(rcopy(ref, ref, s_pair.at[n], r_pair.at[n], (sp, partner)))
+    for send in pair_sends:
+        send.start()
+
+    query_w = (acc4[:, 384:512] * inv).astype(BF16)
 
     @pl.when(has_prev)
     def _():
@@ -217,33 +228,49 @@
         norm = jnp.sum(weight, axis=1, keepdims=True) + jnp.exp2(sink - top)
         outs.append(dot((weight / norm).astype(BF16), values))
     win_out = jnp.concatenate(outs, axis=1).astype(BF16).astype(F32)
-    with_squares(bb, win_out)
-    scaled_w = (win_out * wg_v[...]).astype(BF16)
-    for n in range(4):
-        bb[:, n * 512 : n * 512 + 512] = dot(scaled_w, wo_w[:, n * 512 : n * 512 + 512]).astype(BF16)
-
-    def scatter(buf, dst, ssem, rsem):
+
+    def project_out(result, gain, weight, mix, inbound, buf, dst, slot, ssem, rsem):
+        scaled = (result * gain[...]).astype(BF16)
+        sums = split(jnp.sum(result * result, axis=1, keepdims=True))
+        for core in range(2):
+            for chip in range(NX):
+                rows = slice(32 * chip + 16 * core, 32 * chip + 16 * core + 16)
+                mix[core, 16 * chip : 16 * chip + 16, :128] = scaled[rows]
+                mix[core, 16 * chip : 16 * chip + 16, 128:] = sums[rows]
+        over = rcopy(mix.at[1 - c], inbound, s_pair.at[2 + slot], r_pair.at[2 + slot], (sp, partner))
+        over.start()
+        theirs_w = weight.at[1 - c]
+        rcopy(theirs_w, theirs_w, s_pair.at[0], r_pair.at[slot], (sp, partner)).wait_recv()
+        mine = mix[c, :, :128]
+        own = [dot(mine, weight[c, :, n * 512 : n * 512 + 512]) for n in range(4)]
+        over.wait_recv()
+        theirs = inbound[:, :128]
+        for n in range(4):
+            part = own[n] + dot(theirs, weight[1 - c, :, n * 512 : n * 512 + 512])
+            buf[:, n * 512 : n * 512 + 512] = part.astype(BF16)
+        both = mix[c, :, 128:].astype(F32) + inbound[:, 128:].astype(F32)
+        buf[:, D:] = split(jnp.sum(both, axis=1, keepdims=True))
         sends = []
-        for d in (4, 5, 3, 2, 6, 7, 1):
-            to = (tp + d) % NTP
+        for d in (2, 1, 3):
+            to = (x + d) % NX
             rows = buf.at[pl.ds(pl.multiple_of(to * 16, 16), 16), :]
-            sends.append(rcopy(rows, dst.at[tp], ssem.at[d], rsem.at[tp], (sp, to)))
+            sends.append(rcopy(rows, dst.at[x], ssem.at[d], rsem.at[x], (sp, to * 2 + c)))
         for send in sends:
             send.start()
-        return sends
-
-    win_sends = scatter(bb, rb, s_rb, r_rb)
+        return sends + [over]
+
+    win_sends = project_out(win_out, wg_v, wo_w, mix_b, in_b, bb, rb, 0, s_rb, r_rb)
 
     before, after = (y + NY - 2) % NY, (y + 2) % NY
-    row_of = lambda d: (z * NY + (y + d) % NY, tp)
-    relays = [
-        (before, [(kvb.at[before], 1, r_k.at[before]), (kvb.at[before, 0], 2, r_k4.at[0])]),
-        (after, [(kvb.at[after], NY - 1, r_k.at[after]), (kvb.at[after, 1], NY - 2, r_k4.at[1])]),
-    ]
-    for side, (src, copies) in enumerate(relays):
-        rcopy(kvb.at[src], kvb.at[src], s_k.at[0], r_k.at[src], row_of(1)).wait_recv()
-        for n, (ref, d, rsem) in enumerate(copies):
-            send = rcopy(ref, ref, s_k.at[4 + 2 * side + n], rsem, row_of(d))
+    for plane in range(2):
+        for side, src in enumerate((before, after)):
+            ref = kvb.at[src, plane]
+            rcopy(ref, ref, s_k.at[0], r_k2.at[side, plane], row_of(1)).wait_recv()
+            if side == plane:
+                send = rcopy(ref, ref, s_k.at[6 + side], r_k4.at[side], row_of((2, NY - 2)[side]))
+                send.start()
+                kv_sends.append(send)
+            send = rcopy(ref, ref, s_k.at[8 + 2 * side + plane], r_k3.at[side, plane], row_of((1, NY - 1)[side]))
             send.start()
             kv_sends.append(send)
 
@@ -359,9 +386,13 @@
 
         @pl.when(i == early)
         def _():
-            for d in (1, 5, 3):
-                kv_wait(far[d])
-                spread(far[d])
+            kv_wait(far[1])
+            spread(far[1])
+            for side, src in enumerate((far[5], far[3])):
+                for plane in range(2):
+                    ref = kvb.at[src, plane]
+                    rcopy(ref, ref, s_k.at[0], r_k3.at[side, plane], row_of(1)).wait_recv()
+                spread(src)
             for n in range(2):
                 rcopy(kvb.at[far[4], n], kvb.at[far[4], n], s_k.at[0], r_k4.at[n], row_of(1)).wait_recv()
             spread(far[4])
@@ -393,18 +424,13 @@
     lax.fori_loop(0, z, merge, own_logs)
 
     stick_out = acc_p[...].astype(BF16).astype(F32)
-    with_squares(ab, stick_out)
-    scaled_s = (stick_out * sg_v[...]).astype(BF16)
-    for n in range(4):
-        ab[:, n * 512 : n * 512 + 512] = dot(scaled_s, wo_s[:, n * 512 : n * 512 + 512]).astype(BF16)
-    stick_sends = scatter(ab, ra, s_ra, r_ra)
+    stick_sends = project_out(stick_out, sg_v, wo_s, mix_a, in_a, ab, ra, 1, s_ra, r_ra)
 
     def gathered(buf, dst, rsem):
-        mine = pl.ds(pl.multiple_of(tp * 16, 16), 16)
-        total = buf[mine, :].astype(F32)
-        for d in (1, 2, 6, 7, 3, 5, 4):
-            src = (tp + d) % NTP
-            rcopy(dst.at[src], dst.at[src], s_ra.at[0], rsem.at[src], (sp, src)).wait_recv()
+        total = buf[pl.ds(pl.multiple_of(x * 16, 16), 16), :].astype(F32)
+        for d in (1, 3, 2):
+            src = (x + d) % NX
+            rcopy(dst.at[src], dst.at[src], s_ra.at[0], rsem.at[src], (sp, src * 2 + c)).wait_recv()
             total = total + dst[src].astype(F32)
         scale = lax.rsqrt(jnp.sum(total[:, D:], axis=1, keepdims=True) * (1.0 / 1024) + EPS)
         return total[:, :D] * scale
@@ -414,7 +440,7 @@
     mean = jnp.sum(combined * combined, axis=1, keepdims=True) * (1.0 / D)
     out[...] = (combined * lax.rsqrt(mean + EPS) * post_v[...]).astype(BF16)
 
-    for send in tok_sends + kv_sends + win_sends + stick_sends:
+    for send in tok_sends + kv_sends + pair_sends + win_sends + stick_sends:
         send.wait_send()
 
     @pl.when(has_next)
@@ -446,17 +472,18 @@
     vm = pltpu.VMEM
     scratch = [
         vm((NTP, T, CH), BF16), vm((D, 512), BF16), vm((128, D), BF16),
-        vm((128, D), BF16), vm((128, D), BF16), vm((1, D), F32), vm((1, 128), F32), vm((1, 128), F32), vm((1, D), F32),
+        vm((2, 128, D), BF16), vm((2, 128, D), BF16), vm((1, D), F32), vm((1, 128), F32), vm((1, 128), F32), vm((1, D), F32),
         vm((T, 512), F32), vm((T, 128), F32), vm((T, 128), F32),
         vm((NY, 2, T, 128), BF16), vm(((NZ + 1) * T, 128), BF16), vm((NY, 128, 2 * T), BF16), vm((NY, 2 * T, 128), BF16),
         vm((256, 256), BF16), vm((2, 4 * T, 2 * T), F32), vm((2, 4 * T, 2 * T), BF16), vm((2, 4 * T, 2 * T), F32),
         vm((2, 4 * T, 2 * T), F32), vm((2, 4 * T, 2 * T), BF16),
         vm((NY, (NZ + 3) * T, 128), F32), vm((NY, (NZ + 3) * T, 128), F32), vm((T, 2 * T), jnp.int32),
         vm((T, 128), BF16), vm((T, 128), BF16), vm((NZ, PROWS, 128), BF16), vm((NZ, PROWS, 128), BF16),
-        vm((T, 128), F32), vm((T, PACK), BF16), vm((T, PACK), BF16),
-        vm((NTP, 16, PACK), BF16), vm((NTP, 16, PACK), BF16), pltpu.SMEM((2,), F32), pltpu.SMEM((2,), F32),
-        dma((15,)), dma((7,)), dma((NTP,)), dma((8,)), dma((NY,)), dma((2,)), dma((NZ,)), dma((NZ,)), dma, dma, pltpu.SemaphoreType.REGULAR,
-        dma((NZ,)), dma((NZ,)), dma((NTP,)), dma((NTP,)), dma((NTP,)), dma((NTP,)),
+        vm((T, 128), F32), vm((64, PACK), BF16), vm((64, PACK), BF16),
+        vm((NX, 16, PACK), BF16), vm((NX, 16, PACK), BF16), vm((2, 64, 256), BF16), vm((2, 64, 256), BF16),
+        vm((64, 256), BF16), vm((64, 256), BF16), pltpu.SMEM((2,), F32), pltpu.SMEM((2,), F32),
+        dma((15,)), dma((7,)), dma((NTP,)), dma((12,)), dma((NY,)), dma((2, 2)), dma((2, 2)), dma((2,)), dma((NZ,)), dma((NZ,)), dma, dma, pltpu.SemaphoreType.REGULAR,
+        dma((NZ,)), dma((NZ,)), dma((NX,)), dma((NX,)), dma((NX,)), dma((NX,)), dma((4,)), dma((4,)),
     ]
     return pl.pallas_call(
         kernel,

time: 45.4 us -> 43.9 us (0.967)
  Pallas kernels: 43.4 us -> 42.2 us
    pallas_call x1, Pallas kernels: 43.4 us -> 42.2 us  [shards(): pl.pallas_call(kernel, out_shape=jax.ShapeDtypeStruct((T // NTP, D), BF16...]
where the time goes in v5:
time: 43.9 us; the launch traced here: 43.7 us
  Pallas kernels  42.2 us (96%)
  local copies, waits for them, and re-layouts  1.47 us (3%)
    pallas_call x1, Pallas kernels, shards(): pl.pallas_call(kernel, out_shape=jax.ShapeDtypeStruct((T // NTP, D), BF16...  42.2 us
    unnamed x1, local copies, waits for them, and re-layouts  1.47 us

profile of v5, /device:TPU:257, one launch (start us, length us, event | category | flops | bytes accessed | tf_op | source)
XLA Modules:
  0.0 43.7 jit_solution(10284424224188772994)
XLA Ops:
  0.0 42.2 %shard_map.145 = bf16[16,2048]{1,0:T(8,128)(2,1)} custom-call(bf16[128,256]{1,0:T(8,128)(2,1)} %tok.1, f32[1,2048]{1,0:T(1,128)} %bitcast.8, bf16[2048,128]{1,0:T(8,128)(2,1)} %wqs.1, bf16[2048,128]{1,0:T(8,128)(2,1)} %wks.1, bf16[2048,128]{1,0:T(8,128)(2,1)} %wvs.1, bf16[2048,128]{1,0:T(8,128)(2,1)} %wqw.1, bf16[64,2048]{1,0:T(8,128)(2,1)} %bitcast.6, ...), custom_call_target="tpu_custom_call" | custom-call | tf_op jit(solution)/shard_map/pallas_call | solution.py:488
  42.2 1.5 %copy.17 = bf16[16,2048]{1,0:T(8,128)(2,1)} copy(bf16[16,2048]{1,0:T(8,128)(2,1)} %shard_map.145) | data formatting | bytes 131072

commit v6 on v5

--- a/solution.py
+++ b/solution.py
@@ -17,7 +17,6 @@
 LOG2E = 1.4426950408889634
 EPS = 1e-06
 PACK = D + 128
-PROWS = T + 16
 MESH = pl.DeviceIdType.MESH
 F32 = jnp.float32
 BF16 = jnp.bfloat16
@@ -46,8 +45,8 @@
     out,
     tok_all, w4, w_win, wo_s, wo_w, pre_v, sg_v, wg_v, post_v,
     acc4, acc_w, sq, kvb, qb, kbd, vbd, tri, raw, soft_b, diff, expo, weight_b, parts, logs, offset,
-    wkv, pwkv, pout, prec, acc_p, ab, bb, ra, rb, mix_a, mix_b, in_a, in_b, bias_s, sinks_s,
-    lsem, s_a, r_a, s_k, r_k, r_k2, r_k3, r_k4, s_q, r_q, s_w, r_w, ready, s_p, r_p, s_ra, r_ra, s_rb, r_rb,
+    wkv, pwkv, pout, prec, lout, lrec, acc_p, ab, bb, ra, rb, mix_a, mix_b, in_a, in_b, bias_s, sinks_s,
+    lsem, s_a, r_a, s_k, r_k, r_k2, r_k3, r_k4, s_q, r_q, s_w, r_w, ready, s_p, r_p, s_l, r_l, s_ra, r_ra, s_rb, r_rb,
     s_pair, r_pair,
 ):
     sp = lax.axis_index("sp")
@@ -158,19 +157,6 @@
     lax.fori_loop(0, NTP, feature_step, 0)
     inv = lax.rsqrt(jnp.sum(sq[...], axis=1, keepdims=True) * (1.0 / D) + EPS)
 
-    own_pair = (acc_w[...] * inv).astype(BF16)
-    wkv[...] = own_pair
-
-    @pl.when(ends_row)
-    def _():
-        pl.semaphore_wait(ready, 1)
-
-    win_send = rcopy(wkv, pwkv, s_w, r_w, nxt)
-
-    @pl.when(has_next)
-    def _():
-        win_send.start()
-
     kvb[y, 0] = (acc4[:, 0:128] * inv).T.astype(BF16)
     kvb[y, 1] = (acc4[:, 128:256] * inv).astype(BF16)
     own_kv = kvb.at[y]
@@ -180,10 +166,25 @@
         for side, d in enumerate((2, NY - 2)):
             ref = kvb.at[y, plane]
             kv_sends.append(rcopy(ref, ref, s_k.at[2 * plane + side], r_k2.at[side, plane], row_of(d)))
-    for n, d in enumerate((1, NY - 1)):
-        kv_sends.append(rcopy(own_kv, own_kv, s_k.at[4 + n], r_k.at[y], row_of(d)))
     for send in kv_sends:
         send.start()
+    own_pair = (acc_w[...] * inv).astype(BF16)
+    wkv[...] = own_pair
+
+    @pl.when(ends_row)
+    def _():
+        pl.semaphore_wait(ready, 1)
+
+    win_send = rcopy(wkv, pwkv, s_w, r_w, nxt)
+
+    @pl.when(has_next)
+    def _():
+        win_send.start()
+
+    for n, d in enumerate((1, NY - 1)):
+        send = rcopy(own_kv, own_kv, s_k.at[4 + n], r_k.at[y], row_of(d))
+        send.start()
+        kv_sends.append(send)
     qb[rows_of(z), :] = (acc4[:, 256:384] * (inv * (0.125 * LOG2E))).astype(BF16)
 
     def q_send(i):
@@ -202,6 +203,19 @@
         pair_sends.append(rcopy(ref, ref, s_pair.at[n], r_pair.at[n], (sp, partner)))
     for send in pair_sends:
         send.start()
+
+    before, after = (y + NY - 2) % NY, (y + 2) % NY
+    for plane in range(2):
+        for side, src in enumerate((before, after)):
+            ref = kvb.at[src, plane]
+            rcopy(ref, ref, s_k.at[0], r_k2.at[side, plane], row_of(1)).wait_recv()
+            if side == plane:
+                send = rcopy(ref, ref, s_k.at[6 + side], r_k4.at[side], row_of((2, NY - 2)[side]))
+                send.start()
+                kv_sends.append(send)
+            send = rcopy(ref, ref, s_k.at[8 + 2 * side + plane], r_k3.at[side, plane], row_of((1, NY - 1)[side]))
+            send.start()
+            kv_sends.append(send)
 
     query_w = (acc4[:, 384:512] * inv).astype(BF16)
 
@@ -261,19 +275,6 @@
 
     win_sends = project_out(win_out, wg_v, wo_w, mix_b, in_b, bb, rb, 0, s_rb, r_rb)
 
-    before, after = (y + NY - 2) % NY, (y + 2) % NY
-    for plane in range(2):
-        for side, src in enumerate((before, after)):
-            ref = kvb.at[src, plane]
-            rcopy(ref, ref, s_k.at[0], r_k2.at[side, plane], row_of(1)).wait_recv()
-            if side == plane:
-                send = rcopy(ref, ref, s_k.at[6 + side], r_k4.at[side], row_of((2, NY - 2)[side]))
-                send.start()
-                kv_sends.append(send)
-            send = rcopy(ref, ref, s_k.at[8 + 2 * side + plane], r_k3.at[side, plane], row_of((1, NY - 1)[side]))
-            send.start()
-            kv_sends.append(send)
-
     def spread(j):
         key_t, val = kvb[j, 0], kvb[j, 1]
         zero = jnp.zeros_like(key_t)
@@ -329,13 +330,15 @@
     def p_send(to):
         return rcopy(pout.at[to], prec.at[z], s_p.at[to], r_p.at[z], (to * NY + y, tp))
 
+    def l_send(to):
+        return rcopy(lout.at[to], lrec.at[z], s_l.at[to], r_l.at[z], (to * NY + y, tp))
+
     def give(zq):
         part, (l0, l1) = total_of(zq)
-        pout[zq, :T, :] = part.astype(BF16)
-        h0, h1 = l0.astype(BF16).astype(F32), l1.astype(BF16).astype(F32)
-        row = iota((16, 128), 0)
-        packed = jnp.where(row == 0, h0, jnp.where(row == 1, l0 - h0, jnp.where(row == 2, h1, l1 - h1)))
-        pout[zq, T:, :] = packed.astype(BF16)
+        pout[zq] = part.astype(BF16)
+        lout[zq, 0:1, :] = l0
+        lout[zq, 1:2, :] = l1
+        l_send(zq).start()
         p_send(zq).start()
 
     def unit_step(i, now):
@@ -408,20 +411,22 @@
     lax.fori_loop(0, 2 * query_pairs + 2, two_steps, 0)
 
     own_part, own_logs = total_of(z)
-    acc_p[...] = own_part
-
-    def merge(i, rows):
-        l0, l1 = rows
-        src = z - 1 - i
+
+    def factor_of(rows):
+        spread_rows = [jnp.broadcast_to(jnp.exp2(-row), (64, 128)) for row in rows]
+        return jnp.concatenate(spread_rows, axis=0).T
+
+    acc_p[...] = jnp.zeros_like(acc_p)
+
+    def merge(src, _):
+        rcopy(lout.at[src], lrec.at[src], s_l.at[0], r_l.at[src], (src * NY + y, tp)).wait_recv()
+        factor = factor_of((lrec[src, 0:1, :], lrec[src, 1:2, :]))
         rcopy(pout.at[src], prec.at[src], s_p.at[0], r_p.at[src], (src * NY + y, tp)).wait_recv()
-        factor = jnp.concatenate(
-            [jnp.broadcast_to(jnp.exp2(-l0), (64, 128)), jnp.broadcast_to(jnp.exp2(-l1), (64, 128))], axis=0
-        ).T
-        acc_p[...] += factor * prec[src, :T, :].astype(F32)
-        more = prec[src, T:, :].astype(F32)
-        return l0 + (more[0:1] + more[1:2]), l1 + (more[2:3] + more[3:4])
-
-    lax.fori_loop(0, z, merge, own_logs)
+        acc_p[...] = prec[src].astype(F32) + factor * acc_p[...]
+        return 0
+
+    lax.fori_loop(0, z, merge, 0)
+    acc_p[...] = own_part + factor_of(own_logs) * acc_p[...]
 
     stick_out = acc_p[...].astype(BF16).astype(F32)
     stick_sends = project_out(stick_out, sg_v, wo_s, mix_a, in_a, ab, ra, 1, s_ra, r_ra)
@@ -458,6 +463,7 @@
 
     def p_drain(i, _):
         p_send(NZ - 1 - i).wait_send()
+        l_send(NZ - 1 - i).wait_send()
         return 0
 
     lax.fori_loop(0, NZ - 1 - z, p_drain, 0)
@@ -478,12 +484,13 @@
         vm((256, 256), BF16), vm((2, 4 * T, 2 * T), F32), vm((2, 4 * T, 2 * T), BF16), vm((2, 4 * T, 2 * T), F32),
         vm((2, 4 * T, 2 * T), F32), vm((2, 4 * T, 2 * T), BF16),
         vm((NY, (NZ + 3) * T, 128), F32), vm((NY, (NZ + 3) * T, 128), F32), vm((T, 2 * T), jnp.int32),
-        vm((T, 128), BF16), vm((T, 128), BF16), vm((NZ, PROWS, 128), BF16), vm((NZ, PROWS, 128), BF16),
+        vm((T, 128), BF16), vm((T, 128), BF16), vm((NZ, T, 128), BF16), vm((NZ, T, 128), BF16),
+        vm((NZ, 2, 128), F32), vm((NZ, 2, 128), F32),
         vm((T, 128), F32), vm((64, PACK), BF16), vm((64, PACK), BF16),
         vm((NX, 16, PACK), BF16), vm((NX, 16, PACK), BF16), vm((2, 64, 256), BF16), vm((2, 64, 256), BF16),
         vm((64, 256), BF16), vm((64, 256), BF16), pltpu.SMEM((2,), F32), pltpu.SMEM((2,), F32),
         dma((15,)), dma((7,)), dma((NTP,)), dma((12,)), dma((NY,)), dma((2, 2)), dma((2, 2)), dma((2,)), dma((NZ,)), dma((NZ,)), dma, dma, pltpu.SemaphoreType.REGULAR,
-        dma((NZ,)), dma((NZ,)), dma((NX,)), dma((NX,)), dma((NX,)), dma((NX,)), dma((4,)), dma((4,)),
+        dma((NZ,)), dma((NZ,)), dma((NZ,)), dma((NZ,)), dma((NX,)), dma((NX,)), dma((NX,)), dma((NX,)), dma((4,)), dma((4,)),
     ]
     return pl.pallas_call(
         kernel,

time: 43.9 us -> 43.5 us (level)
  no operation moved by 1% of the time
where the time goes in v6:
time: 43.5 us; the launch traced here: 43.3 us
  Pallas kernels  41.9 us (96%)
  local copies, waits for them, and re-layouts  1.47 us (3%)
    pallas_call x1, Pallas kernels, shards(): pl.pallas_call(kernel, out_shape=jax.ShapeDtypeStruct((T // NTP, D), BF16...  41.9 us
    unnamed x1, local copies, waits for them, and re-layouts  1.47 us

profile of v6, /device:TPU:257, one launch (start us, length us, event | category | flops | bytes accessed | tf_op | source)
XLA Modules:
  0.0 43.3 jit_solution(14391495163926950627)
XLA Ops:
  0.0 41.9 %shard_map.145 = bf16[16,2048]{1,0:T(8,128)(2,1)} custom-call(bf16[128,256]{1,0:T(8,128)(2,1)} %tok.1, f32[1,2048]{1,0:T(1,128)} %bitcast.8, bf16[2048,128]{1,0:T(8,128)(2,1)} %wqs.1, bf16[2048,128]{1,0:T(8,128)(2,1)} %wks.1, bf16[2048,128]{1,0:T(8,128)(2,1)} %wvs.1, bf16[2048,128]{1,0:T(8,128)(2,1)} %wqw.1, bf16[64,2048]{1,0:T(8,128)(2,1)} %bitcast.6, ...), custom_call_target="tpu_custom_call" | custom-call | tf_op jit(solution)/shard_map/pallas_call | solution.py:495
  41.9 1.5 %copy.17 = bf16[16,2048]{1,0:T(8,128)(2,1)} copy(bf16[16,2048]{1,0:T(8,128)(2,1)} %shard_map.145) | data formatting | bytes 131072

commit v7 on v6

--- a/solution.py
+++ b/solution.py
@@ -168,6 +168,17 @@
             kv_sends.append(rcopy(ref, ref, s_k.at[2 * plane + side], r_k2.at[side, plane], row_of(d)))
     for send in kv_sends:
         send.start()
+    qb[rows_of(z), :] = (acc4[:, 256:384] * (inv * (0.125 * LOG2E))).astype(BF16)
+
+    def q_send(i):
+        return rcopy(qb.at[rows_of(z), :], qb.at[rows_of(z), :], s_q.at[i], r_q.at[z], (i * NY + y, tp))
+
+    def q_start(i, _):
+        q_send(i).start()
+        return 0
+
+    lax.fori_loop(0, z, q_start, 0)
+
     own_pair = (acc_w[...] * inv).astype(BF16)
     wkv[...] = own_pair
 
@@ -185,17 +196,6 @@
         send = rcopy(own_kv, own_kv, s_k.at[4 + n], r_k.at[y], row_of(d))
         send.start()
         kv_sends.append(send)
-    qb[rows_of(z), :] = (acc4[:, 256:384] * (inv * (0.125 * LOG2E))).astype(BF16)
-
-    def q_send(i):
-        return rcopy(qb.at[rows_of(z), :], qb.at[rows_of(z), :], s_q.at[i], r_q.at[z], (i * NY + y, tp))
-
-    def q_start(i, _):
-        q_send(i).start()
-        return 0
-
-    lax.fori_loop(0, z, q_start, 0)
-
     for load in loads[8:]:
         load.wait()
     pair_sends = []
@@ -296,7 +296,8 @@
     def unit(i):
         at = jnp.clip(i, 0, units - 1)
         mid, rest = at - 2 * early, jnp.maximum(at - 4 * early, 0)
-        p = jnp.where(mid < 0, at // 2, jnp.where(mid < 2 * early, early - 1 - mid // 2, early + rest // 4))
+        turn = jnp.where(z == 3, mid // 2, early - 1 - mid // 2)
+        p = jnp.where(mid < 0, at // 2, jnp.where(mid < 2 * early, turn, early + rest // 4))
         k = jnp.where(mid < 0, at % 2, jnp.where(mid < 2 * early, 2 + mid % 2, rest % 4))
         real = (i >= 0) & (i < units)
         first = jnp.where(k == 0, y, jnp.where(k == 1, after, jnp.where(k == 2, far[1], far[3])))
@@ -341,29 +342,33 @@
         l_send(zq).start()
         p_send(zq).start()
 
-    def unit_step(i, now):
+    def unit_step(i, now, stages=5):
         later = 1 - now
         _, _, _, pair_d, rows_d = unit(i - 4)
-        p, _, _, pair, _ = unit(i)
         for half, j in zip(halves, pair_d):
             parts[j, rows_d, :] = dot(weight_b[now, half, :], vbd[j])
-        weight_b[later] = jnp.exp2(expo[now]).astype(BF16)
-        expo[later] = diff[now] - dot(soft_b[now], tri[...])
-        _, _, _, pair_b, rows_b = unit(i - 1)
-        for half, j in zip(halves, pair_b):
-            score = raw[now, half, :] + bias_row
-            soft = jnp.maximum(score, jnp.log(1.0 + jnp.exp2(jnp.minimum(score, 126.0))) * LOG2E)
-            diff[later, half, :] = score - soft
-            soft_b[later, half, :] = soft.astype(BF16)
-            sum0 = jnp.sum(soft[:, :T], axis=1, keepdims=True)
-            sum1 = jnp.sum(soft[:, T:], axis=1, keepdims=True)
-            logs[j, rows_b, :] = jnp.where(in_head0, sum0, sum1)
-        own_rows = rows_of(jnp.minimum(z + 2 * p, NZ - 1), 2)
-        for half, j in zip(halves, pair):
-            score = dot(qb[own_rows, :], kbd[j])
-            limit = jnp.where(p == 0, (y - j) * T, NY * T)
-            raw[later, pl.ds(half.start, T), :] = jnp.where(offset[...] < limit, score[:T], -1e30)
-            raw[later, pl.ds(half.start + T, T), :] = score[T:]
+        if stages >= 2:
+            weight_b[later] = jnp.exp2(expo[now]).astype(BF16)
+        if stages >= 3:
+            expo[later] = diff[now] - dot(soft_b[now], tri[...])
+        if stages >= 4:
+            _, _, _, pair_b, rows_b = unit(i - 1)
+            for half, j in zip(halves, pair_b):
+                score = raw[now, half, :] + bias_row
+                soft = jnp.maximum(score, jnp.log(1.0 + jnp.exp2(jnp.minimum(score, 126.0))) * LOG2E)
+                diff[later, half, :] = score - soft
+                soft_b[later, half, :] = soft.astype(BF16)
+                sum0 = jnp.sum(soft[:, :T], axis=1, keepdims=True)
+                sum1 = jnp.sum(soft[:, T:], axis=1, keepdims=True)
+                logs[j, rows_b, :] = jnp.where(in_head0, sum0, sum1)
+        if stages >= 5:
+            p, _, _, pair, _ = unit(i)
+            own_rows = rows_of(jnp.minimum(z + 2 * p, NZ - 1), 2)
+            limit_of = lambda j: jnp.where(p == 0, (y - j) * T, NY * T)
+            for half, j in zip(halves, pair):
+                score = dot(qb[own_rows, :], kbd[j])
+                raw[later, pl.ds(half.start, T), :] = jnp.where(offset[...] < limit_of(j), score[:T], -1e30)
+                raw[later, pl.ds(half.start + T, T), :] = score[T:]
 
     def give_done(i):
         p_d, k_d, real_d, _, _ = unit(i)
@@ -408,7 +413,13 @@
     spread(y)
     spread(before)
     spread(after)
-    lax.fori_loop(0, 2 * query_pairs + 2, two_steps, 0)
+    lax.fori_loop(0, 2 * query_pairs, two_steps, 0)
+    unit_step(units, 0, 4)
+    unit_step(units + 1, 1, 3)
+    give_done(units - 3)
+    unit_step(units + 2, 0, 2)
+    unit_step(units + 3, 1, 1)
+    give_done(units - 1)
 
     own_part, own_logs = total_of(z)
 

time: 43.5 us -> 43.7 us (level)
  the two profiles are of different devices: /device:TPU:257 before, /device:TPU:385 now
where the time goes in v7:
time: 43.7 us; the launch traced here: 43.6 us
  Pallas kernels  42.1 us (96%)
  local copies, waits for them, and re-layouts  1.47 us (3%)
    pallas_call x1, Pallas kernels, shards(): pl.pallas_call(kernel, out_shape=jax.ShapeDtypeStruct((T // NTP, D), BF16...  42.1 us
    unnamed x1, local copies, waits for them, and re-layouts  1.47 us

profile of v7, /device:TPU:385, one launch (start us, length us, event | category | flops | bytes accessed | tf_op | source)
XLA Modules:
  0.0 43.6 jit_solution(7642193542223250850)
XLA Ops:
  0.0 42.1 %shard_map.145 = bf16[16,2048]{1,0:T(8,128)(2,1)} custom-call(bf16[128,256]{1,0:T(8,128)(2,1)} %tok.1, f32[1,2048]{1,0:T(1,128)} %bitcast.8, bf16[2048,128]{1,0:T(8,128)(2,1)} %wqs.1, bf16[2048,128]{1,0:T(8,128)(2,1)} %wks.1, bf16[2048,128]{1,0:T(8,128)(2,1)} %wvs.1, bf16[2048,128]{1,0:T(8,128)(2,1)} %wqw.1, bf16[64,2048]{1,0:T(8,128)(2,1)} %bitcast.6, ...), custom_call_target="tpu_custom_call" | custom-call | tf_op jit(solution)/shard_map/pallas_call | solution.py:506
  42.1 1.5 %copy.17 = bf16[16,2048]{1,0:T(8,128)(2,1)} copy(bf16[16,2048]{1,0:T(8,128)(2,1)} %shard_map.145) | data formatting | bytes 131072

commit v8 on v7

--- a/solution.py
+++ b/solution.py
@@ -296,7 +296,7 @@
     def unit(i):
         at = jnp.clip(i, 0, units - 1)
         mid, rest = at - 2 * early, jnp.maximum(at - 4 * early, 0)
-        turn = jnp.where(z == 3, mid // 2, early - 1 - mid // 2)
+        turn = early - 1 - mid // 2
         p = jnp.where(mid < 0, at // 2, jnp.where(mid < 2 * early, turn, early + rest // 4))
         k = jnp.where(mid < 0, at % 2, jnp.where(mid < 2 * early, 2 + mid % 2, rest % 4))
         real = (i >= 0) & (i < units)

time: 43.7 us -> 43.5 us (level)
  the two profiles are of different devices: /device:TPU:385 before, /device:TPU:257 now
where the time goes in v8:
time: 43.5 us; the launch traced here: 43.4 us
  Pallas kernels  41.9 us (96%)
  local copies, waits for them, and re-layouts  1.47 us (3%)
    pallas_call x1, Pallas kernels, shards(): pl.pallas_call(kernel, out_shape=jax.ShapeDtypeStruct((T // NTP, D), BF16...  41.9 us
    unnamed x1, local copies, waits for them, and re-layouts  1.47 us

profile of v8, /device:TPU:257, one launch (start us, length us, event | category | flops | bytes accessed | tf_op | source)
XLA Modules:
  0.0 43.4 jit_solution(12168701514320561276)
XLA Ops:
  0.0 41.9 %shard_map.145 = bf16[16,2048]{1,0:T(8,128)(2,1)} custom-call(bf16[128,256]{1,0:T(8,128)(2,1)} %tok.1, f32[1,2048]{1,0:T(1,128)} %bitcast.8, bf16[2048,128]{1,0:T(8,128)(2,1)} %wqs.1, bf16[2048,128]{1,0:T(8,128)(2,1)} %wks.1, bf16[2048,128]{1,0:T(8,128)(2,1)} %wvs.1, bf16[2048,128]{1,0:T(8,128)(2,1)} %wqw.1, bf16[64,2048]{1,0:T(8,128)(2,1)} %bitcast.6, ...), custom_call_target="tpu_custom_call" | custom-call | tf_op jit(solution)/shard_map/pallas_call | solution.py:506
  41.9 1.5 %copy.17 = bf16[16,2048]{1,0:T(8,128)(2,1)} copy(bf16[16,2048]{1,0:T(8,128)(2,1)} %shard_map.145) | data formatting | bytes 131072
